TPU v7x, 32 devices: a whole 2x2x4 slice. The times are simulated.
32 devices in a mesh: sp: 16 (over z, y, x), tp: 2 (over core).
Axes of the slice: x: 2, y: 2, z: 4, core: 2. Of those that a mesh axis runs over, the one named last changes fastest.
Arguments:
- queries: bfloat16 [2048, 1024], P('sp', 'tp'), may hold values from -6 to 6
- attn_out: bfloat16 [2048, 1024], P('sp', 'tp'), may hold values from -6 to 6
- out_grad: bfloat16 [2048, 1024], P('sp', 'tp'), may hold values from -384 to 384
- row_lse: float32 [2048, 8], P('sp', 'tp'), may hold values from 9.5 to 12.5
- source: bfloat16 [8192, 4096], P('sp', 'tp'), may hold values from -6 to 6
- saved_keys: bfloat16 [8192, 256], P('sp'), may hold values from -6 to 6
- saved_values: bfloat16 [8192, 256], P('sp'), may hold values from -6 to 6
- key_weight: bfloat16 [4096, 256], P('tp'), may hold values from -0.09375 to 0.09375
- value_weight: bfloat16 [4096, 256], P('tp'), may hold values from -0.09375 to 0.09375
Outputs:
- query_grad: float32 [2048, 1024], P('sp', 'tp')
- source_grad: float32 [8192, 4096], P('sp', 'tp')
- key_grad: float32 [256, 4096], P('sp', 'tp')
All inputs are finite; a program needn't handle non-finite values.
Results may differ from a plain program's by a relative error of at most 0.012.
Values may be sent and summed in bfloat16 or wider, within the bound.
A program may use at most 64 MiB of HBM per device.

v0:
```python
import functools
import math

import jax
import jax.numpy as jnp
from jax import lax
from jax.experimental import pallas as pl
from jax.experimental.pallas import tpu as pltpu
from jax.sharding import PartitionSpec as P

HEADS = 8
KV_HEADS = 2
HEAD_DIM = 128
LOG2E = 1.0 / math.log(2.0)
MESH = pl.DeviceIdType.MESH
F32 = jnp.float32
BF16 = jnp.bfloat16


def dot_nt(left, right, precision=None):
    return lax.dot_general(
        left, right, (((1,), (1,)), ((), ())), preferred_element_type=F32, precision=precision
    )


def dot_tn(left, right):
    return lax.dot_general(left, right, (((0,), (0,)), ((), ())), preferred_element_type=F32)


def dot_nn(left, right):
    return jnp.dot(left, right, preferred_element_type=F32)


def kernel(
    tgt_n, src_n, key_n, tp_n, src_total,
    q_ref, o_ref, d_ref, lse_ref, key_ref, value_ref, source_ref,
    dq_ref, kv_ref, kg_ref,
    qd, stats, kvs, dk, dv, dq_acc, dq_out, dq_in, dq_via, g_out, g_in, tp_own, tp_in,
    src, a_out, a_in, a2_own, a2_out, a2_in, b_out, b_in, b2_own, b2_out, b2_in,
    copy_sem, qd_s, qd_r, rq_s, st_s, st_r, kv_s, kv_r, rkv_s, dq_s, dq_r, via_r, g_s, g_r, tp_s, tp_r,
    a_s, a_r, a2_s, a2_r, b_s, b_r, b2_s, b2_r,
):
    sp = lax.axis_index("sp")
    tp = lax.axis_index("tp")
    sp_n = tgt_n * src_n
    t_hi, t_lo = sp // (2 * src_n), sp % 2
    me_t = t_hi * 2 + t_lo
    me_s = (sp // 2) % src_n
    s_hi, s_lo = me_s // 2, me_s % 2
    near_t, near_s = t_hi * 2 + 1 - t_lo, s_hi * 2 + 1 - s_lo
    t_his = [lax.rem(t_hi + k, tgt_n // 2) for k in range(1, tgt_n // 2)]
    s_his = [lax.rem(s_hi + k, src_n // 2) for k in range(1, src_n // 2)]
    far_t = [hi * 2 + t_lo for hi in t_his]
    diag_t = [hi * 2 + 1 - t_lo for hi in t_his]
    far_s = [hi * 2 + s_lo for hi in s_his]
    diag_s = [hi * 2 + 1 - s_lo for hi in s_his]
    t_peers = far_t + [near_t] + diag_t
    s_peers = far_s + [near_s] + diag_s
    key_m = sp_n // key_n
    me_o, me_i = sp // key_n, sp % key_n
    o_peers = [lax.rem(me_o + k, key_m) for k in range(1, key_m)]
    i_peers = [lax.rem(me_i + k, key_n) for k in range(1, key_n)]
    tp_peers = [lax.rem(tp + k, tp_n) for k in range(1, tp_n)]
    rows = q_ref.shape[0]
    heads = q_ref.shape[1] // HEAD_DIM
    chunks = stats.shape[1]
    per_chunk = heads // chunks
    src_rows = key_ref.shape[0]
    per_key = HEADS // KV_HEADS
    scale = 1.0 / math.sqrt(HEAD_DIM)
    kv_col = pl.multiple_of(tp * heads // per_key * HEAD_DIM, HEAD_DIM)

    def t_dev(t):
        return {"sp": t // 2 * (2 * src_n) + me_s * 2 + t % 2, "tp": tp}

    def s_dev(s):
        return {"sp": t_hi * (2 * src_n) + s * 2 + t_lo, "tp": tp}

    def o_dev(o):
        return {"sp": o * key_n + me_i, "tp": tp}

    def i_dev(i):
        return {"sp": me_o * key_n + i, "tp": tp}

    def tp_dev(p):
        return {"sp": sp, "tp": p}

    def remote(source, target, send, recv, device):
        return pltpu.make_async_remote_copy(
            src_ref=source, dst_ref=target, send_sem=send, recv_sem=recv,
            device_id=device, device_id_type=MESH,
        )

    load = pltpu.make_async_copy(source_ref, src, copy_sem)
    load.start()
    barrier = pltpu.get_barrier_semaphore()
    for k in range(1, sp_n):
        pl.semaphore_signal(
            barrier, inc=1, device_id={"sp": lax.rem(sp + k, sp_n), "tp": tp}, device_id_type=MESH
        )
    for p in tp_peers:
        pl.semaphore_signal(barrier, inc=1, device_id=tp_dev(p), device_id_type=MESH)
    ones = jnp.ones((8, HEAD_DIM), F32)
    for h in range(heads):
        cols = pl.ds(h * HEAD_DIM, HEAD_DIM)
        c, span = h // per_chunk, pl.ds(h % per_chunk * rows, rows)
        prod = d_ref[:, cols].astype(F32) * o_ref[:, cols].astype(F32)
        delta = dot_nt(ones, prod, lax.Precision.HIGHEST)
        stats[me_t, c, 0:1, span] = lse_ref[h : h + 1, :] * LOG2E
        stats[me_t, c, 1:2, span] = delta[0:1, :]
    kvs[me_s, 0] = key_ref[:, pl.ds(kv_col, HEAD_DIM)]
    kvs[me_s, 1] = value_ref[:, pl.ds(kv_col, HEAD_DIM)]
    qd[me_t, 0] = q_ref[...]
    qd[me_t, 1] = d_ref[...]
    dk[...] = jnp.zeros_like(dk)
    dv[...] = jnp.zeros_like(dv)
    dq_acc[...] = jnp.zeros_like(dq_acc)
    pl.semaphore_wait(barrier, sp_n + tp_n - 2)

    def send_q(t):
        for i, ref in enumerate((q_ref, d_ref)):
            remote(ref, qd.at[me_t, i], qd_s.at[t, i], qd_r.at[me_t, i], t_dev(t)).start()

    for s in far_s + [near_s]:
        remote(kvs.at[me_s], kvs.at[me_s], kv_s.at[s], kv_r.at[me_s], s_dev(s)).start()
    for t in far_t + [near_t]:
        send_q(t)

    for t in t_peers:
        remote(stats.at[me_t], stats.at[me_t], st_s.at[t], st_r.at[me_t], t_dev(t)).start()

    def stack(t, i, c):
        low = c * per_chunk
        return jnp.concatenate(
            [
                qd[t, i, :, pl.ds(pl.multiple_of((low + h) * HEAD_DIM, HEAD_DIM), HEAD_DIM)]
                for h in range(per_chunk)
            ],
            axis=0,
        )

    def tile(t, s):
        def body(c, carry):
            q, d = stack(t, 0, c), stack(t, 1, c)
            k, v = kvs[s, 0], kvs[s, 1]
            scores = dot_nt(k, q)
            probs = jnp.exp2(scores * (scale * LOG2E) - stats[t, c, 0:1, :])
            dprobs = dot_nt(v, d)
            dscores = (probs * (dprobs - stats[t, c, 1:2, :])).astype(BF16)
            dv[s] += dot_nn(probs.astype(BF16), d)
            dk[s] += dot_nn(dscores, q)
            dq_acc[t, c] += dot_tn(dscores, k)
            return carry

        lax.fori_loop(0, chunks, body, 0)

    def got_q(t, c):
        remote(qd.at[t, c], qd.at[t, c], qd_s.at[t, c], qd_r.at[t, c], t_dev(t)).wait_recv()

    def got_stats(t):
        remote(stats.at[t], stats.at[t], st_s.at[t], st_r.at[t], t_dev(t)).wait_recv()

    def got_kv(s):
        remote(kvs.at[s], kvs.at[s], kv_s.at[s], kv_r.at[s], s_dev(s)).wait_recv()

    def relay_q(t, c):
        return remote(
            qd.at[t, c], qd.at[t, c], rq_s.at[t, c], qd_r.at[t, c], t_dev(near_t)
        )

    def relay_kv(s):
        return remote(kvs.at[s], kvs.at[s], rkv_s.at[s], kv_r.at[s], s_dev(near_s))

    def dq_copy(t):
        return remote(dq_out.at[t], dq_in.at[me_t], dq_s.at[t], dq_r.at[me_t], t_dev(t))

    def send_g(s, i):
        g_out[s, i] = dv[s].astype(BF16) if i else (dk[s] * scale).astype(BF16)
        remote(
            g_out.at[s, i], g_in.at[me_s, i], g_s.at[s, i], g_r.at[me_s, i], s_dev(s)
        ).start()

    tile(me_t, me_s)
    for s in far_s:
        got_kv(s)
        relay_kv(s).start()
    got_kv(near_s)
    tile(me_t, near_s)
    for c in range(2):
        for t in far_t:
            got_q(t, c)
            relay_q(t, c).start()
        if c == 0:
            for s in far_s:
                tile(me_t, s)
            for c2 in range(2):
                got_q(near_t, c2)
            got_stats(near_t)
    for s in [me_s, near_s] + far_s:
        tile(near_t, s)
    for t in far_t:
        got_stats(t)
        for s in [me_s, near_s] + far_s:
            tile(t, s)
    for s in diag_s:
        got_kv(s)
        for t in [near_t] + far_t + [me_t]:
            tile(t, s)
    dq_out[near_t] = (dq_acc[near_t] * scale).astype(BF16)
    dq_copy(near_t).start()
    for n, t in enumerate(diag_t):
        for c in range(2):
            got_q(t, c)
        got_stats(t)
        for s in far_s + diag_s + [near_s]:
            tile(t, s)
            if n == len(diag_t) - 1:
                send_g(s, 0)
        if n == len(diag_t) - 1:
            for s in far_s + diag_s + [near_s]:
                send_g(s, 1)
        tile(t, me_s)
        dq_out[t] = (dq_acc[t] * scale).astype(BF16)
        remote(dq_out.at[t], dq_via.at[t], dq_s.at[t], via_r.at[t], t_dev(near_t)).start()
    for t in far_t:
        remote(dq_out.at[t], dq_via.at[t], dq_s.at[t], via_r.at[t], t_dev(near_t)).wait_recv()
        dq_out[t] = (dq_acc[t] * scale + dq_via[t].astype(F32)).astype(BF16)
        dq_copy(t).start()

    def reduce_g(i):
        total = dv[me_s] if i else dk[me_s] * scale
        for s in s_peers:
            remote(
                g_in.at[s, i], g_in.at[s, i], g_s.at[s, i], g_r.at[s, i], s_dev(s)
            ).wait_recv()
            total += g_in[s, i].astype(F32)
        tp_own[i] = total.astype(BF16)
        for p in tp_peers:
            remote(
                tp_own.at[i], tp_in.at[tp, i], tp_s.at[p, i], tp_r.at[tp, i], tp_dev(p)
            ).start()
        tp_in[tp, i] = tp_own[i]

    def gather_g(i):
        for p in tp_peers:
            remote(
                tp_in.at[p, i], tp_in.at[p, i], tp_s.at[p, i], tp_r.at[p, i], tp_dev(p)
            ).wait_recv()
        for g in range(KV_HEADS):
            owners = [p for p in range(tp_n) if p * heads // per_key == g]
            half = tp_in[owners[0], i]
            if len(owners) > 1:
                total = half.astype(F32)
                for p in owners[1:]:
                    total += tp_in[p, i].astype(F32)
                half = total.astype(BF16)
            kv_ref[:, pl.ds((i * KV_HEADS + g) * HEAD_DIM, HEAD_DIM)] = half

    reduce_g(0)
    load.wait()
    gather_g(0)
    part = a2_own.shape[1]
    cut = a2_own.shape[2]
    key_half = kv_ref[:, 0 : KV_HEADS * HEAD_DIM]
    w_scale = 1.0 / math.sqrt(src_total)
    partial = dot_tn(key_half, src[...]) * w_scale
    for o in range(key_m):
        for i in range(key_n):
            low = (o * key_n + i) * part
            block = partial[low : low + part].astype(BF16)
            a_out[i, o] = block[:, :cut]
            b_out[o, i] = block[:, cut:]
    for i in i_peers:
        remote(a_out.at[i], a_in.at[me_i], a_s.at[i], a_r.at[me_i], i_dev(i)).start()
    for o in o_peers:
        remote(b_out.at[o], b_in.at[me_o], b_s.at[o], b_r.at[me_o], o_dev(o)).start()

    reduce_g(1)
    gather_g(1)
    dq_total = dq_acc[me_t] * scale
    for t in [near_t] + far_t:
        remote(dq_in.at[t], dq_in.at[t], dq_s.at[t], dq_r.at[t], t_dev(t)).wait_recv()
        dq_total += dq_in[t].astype(F32)
    for h in range(heads):
        low = h % per_chunk * rows
        dq_ref[:, h * HEAD_DIM : (h + 1) * HEAD_DIM] = dq_total[h // per_chunk, low : low + rows]

    total = b_out[me_o].astype(F32)
    for o in o_peers:
        remote(b_in.at[o], b_in.at[o], b_s.at[o], b_r.at[o], o_dev(o)).wait_recv()
        total += b_in[o].astype(F32)
    b2_own[...] = total
    b2_out[...] = total.astype(BF16)
    for i in i_peers:
        remote(b2_out.at[i], b2_in.at[me_i], b2_s.at[i], b2_r.at[me_i], i_dev(i)).start()
    total = a_out[me_i].astype(F32)
    for i in i_peers:
        remote(a_in.at[i], a_in.at[i], a_s.at[i], a_r.at[i], i_dev(i)).wait_recv()
        total += a_in[i].astype(F32)
    a2_own[...] = total
    a2_out[...] = total.astype(BF16)
    for o in o_peers:
        remote(a2_out.at[o], a2_in.at[me_o], a2_s.at[o], a2_r.at[me_o], o_dev(o)).start()
    total = b2_own[me_i]
    for i in i_peers:
        remote(b2_in.at[i], b2_in.at[i], b2_s.at[i], b2_r.at[i], i_dev(i)).wait_recv()
        total += b2_in[i].astype(F32)
    kg_ref[:, cut:] = total
    total = a2_own[me_o]
    for o in o_peers:
        remote(a2_in.at[o], a2_in.at[o], a2_s.at[o], a2_r.at[o], o_dev(o)).wait_recv()
        total += a2_in[o].astype(F32)
    kg_ref[:, :cut] = total

    for t in far_t + [near_t]:
        for c in range(2):
            remote(qd.at[t, c], qd.at[t, c], qd_s.at[t, c], qd_r.at[t, c], t_dev(t)).wait_send()
    for t in far_t:
        for c in range(2):
            relay_q(t, c).wait_send()
    for t in t_peers:
        remote(stats.at[t], stats.at[t], st_s.at[t], st_r.at[t], t_dev(t)).wait_send()
        remote(dq_out.at[t], dq_in.at[t], dq_s.at[t], dq_r.at[t], t_dev(t)).wait_send()
    for s in far_s + [near_s]:
        remote(kvs.at[s], kvs.at[s], kv_s.at[s], kv_r.at[s], s_dev(s)).wait_send()
    for s in far_s:
        relay_kv(s).wait_send()
    for s in s_peers:
        for i in range(2):
            remote(
                g_out.at[s, i], g_in.at[s, i], g_s.at[s, i], g_r.at[s, i], s_dev(s)
            ).wait_send()
    for i in i_peers:
        remote(a_out.at[i], a_in.at[i], a_s.at[i], a_r.at[i], i_dev(i)).wait_send()
        remote(b2_out.at[i], b2_in.at[i], b2_s.at[i], b2_r.at[i], i_dev(i)).wait_send()
    for o in o_peers:
        remote(b_out.at[o], b_in.at[o], b_s.at[o], b_r.at[o], o_dev(o)).wait_send()
        remote(a2_out.at[o], a2_in.at[o], a2_s.at[o], a2_r.at[o], o_dev(o)).wait_send()
    for p in tp_peers:
        for i in range(2):
            remote(
                tp_own.at[i], tp_in.at[p, i], tp_s.at[p, i], tp_r.at[p, i], tp_dev(p)
            ).wait_send()


def shards(
    tgt_n, src_n, tp_n,
    queries, attn_out, out_grad, row_lse, source, saved_keys, saved_values, key_weight, value_weight
):
    heads = row_lse.shape[1]
    rows, width = queries.shape
    src_rows, columns = source.shape
    kv_width = KV_HEADS * HEAD_DIM
    sp_n = tgt_n * src_n
    part = kv_width // sp_n
    key_n, key_m = src_n, tgt_n
    chunks = math.gcd(heads, 2)
    stacked = heads // chunks * rows
    cut = (2 * columns // 3 + 127) // 128 * 128
    rest = columns - cut
    dma = pltpu.SemaphoreType.DMA
    vmem = pl.BlockSpec(memory_space=pltpu.VMEM)
    scratch = [
        pltpu.VMEM((tgt_n, 2, rows, width), BF16),
        pltpu.VMEM((tgt_n, chunks, 8, stacked), F32),
        pltpu.VMEM((src_n, 2, src_rows, HEAD_DIM), BF16),
        pltpu.VMEM((src_n, src_rows, HEAD_DIM), F32),
        pltpu.VMEM((src_n, src_rows, HEAD_DIM), F32),
        pltpu.VMEM((tgt_n, chunks, stacked, HEAD_DIM), F32),
        pltpu.VMEM((tgt_n, chunks, stacked, HEAD_DIM), BF16),
        pltpu.VMEM((tgt_n, chunks, stacked, HEAD_DIM), BF16),
        pltpu.VMEM((tgt_n, chunks, stacked, HEAD_DIM), BF16),
        pltpu.VMEM((src_n, 2, src_rows, HEAD_DIM), BF16),
        pltpu.VMEM((src_n, 2, src_rows, HEAD_DIM), BF16),
        pltpu.VMEM((2, src_rows, HEAD_DIM), BF16),
        pltpu.VMEM((tp_n, 2, src_rows, HEAD_DIM), BF16),
        pltpu.VMEM((src_rows, columns), BF16),
        pltpu.VMEM((key_n, key_m, part, cut), BF16),
        pltpu.VMEM((key_n, key_m, part, cut), BF16),
        pltpu.VMEM((key_m, part, cut), F32),
        pltpu.VMEM((key_m, part, cut), BF16),
        pltpu.VMEM((key_m, part, cut), BF16),
        pltpu.VMEM((key_m, key_n, part, rest), BF16),
        pltpu.VMEM((key_m, key_n, part, rest), BF16),
        pltpu.VMEM((key_n, part, rest), F32),
        pltpu.VMEM((key_n, part, rest), BF16),
        pltpu.VMEM((key_n, part, rest), BF16),
        dma,
    ]
    for shape in (
        (tgt_n, 2), (tgt_n, 2), (tgt_n, 2), (tgt_n,), (tgt_n,),
        (src_n,), (src_n,), (src_n,), (tgt_n,), (tgt_n,), (tgt_n,), (src_n, 2), (src_n, 2),
        (tp_n, 2), (tp_n, 2), (key_n,), (key_n,), (key_m,), (key_m,),
        (key_m,), (key_m,), (key_n,), (key_n,),
    ):
        scratch.append(dma(shape))
    query_grad, kv_half, key_grad = pl.pallas_call(
        functools.partial(kernel, tgt_n, src_n, key_n, tp_n, src_rows * sp_n),
        out_shape=(
            jax.ShapeDtypeStruct((rows, width), F32),
            jax.ShapeDtypeStruct((src_rows, 2 * kv_width), BF16),
            jax.ShapeDtypeStruct((part, columns), F32),
        ),
        in_specs=[vmem] * 6 + [pl.BlockSpec(memory_space=pl.ANY)],
        out_specs=(vmem, vmem, vmem),
        scratch_shapes=scratch,
        compiler_params=pltpu.CompilerParams(
            collective_id=0, has_side_effects=True, vmem_limit_bytes=60 * 2**20
        ),
        name="attention_grads",
    )(queries, attn_out, out_grad, row_lse.T, saved_keys, saved_values, source)
    source_grad = dot_nt(kv_half[:, :kv_width], key_weight) + dot_nt(
        kv_half[:, kv_width:], value_weight
    )
    return (query_grad, source_grad, key_grad)


def solution(mesh):
    sp_n, tp_n = mesh.shape["sp"], mesh.shape["tp"]
    src_n = 2 ** (int(math.log2(sp_n)) // 2)
    in_specs = (
        P("sp", "tp"),
        P("sp", "tp"),
        P("sp", "tp"),
        P("sp", "tp"),
        P("sp", "tp"),
        P("sp", None),
        P("sp", None),
        P("tp", None),
        P("tp", None),
    )
    out_specs = (P("sp", "tp"), P("sp", "tp"), P("sp", "tp"))
    return jax.shard_map(
        functools.partial(shards, sp_n // src_n, src_n, tp_n),
        mesh=mesh, in_specs=in_specs, out_specs=out_specs, check_vma=False,
    )
```

profile of v0, /device:TPU:0, one launch (start us, length us, event | category | flops | bytes accessed | tf_op | source)
XLA Modules:
  0.0 69.3 jit_solution(11537138999329517832)
XLA Ops:
  0.6 0.0 copy-start
  0.6 0.0 copy-start.1
  0.7 62.7 %attention_grads.1 = (f32[128,512]{1,0:T(8,128)}, bf16[512,512]{1,0:T(8,128)(2,1)}, f32[16,2048]{1,0:T(8,128)}) custom-call(bf16[128,512]{1,0:T(8,128)(2,1)} %q_ref.1, bf16[128,512]{1,0:T(8,128)(2,1)} %o_ref.1, bf16[128,512]{1,0:T(8,128)(2,1)} %d_ref.1, f32[4,128]{1,0:T(4,128)} %bitcast.3, bf16[512,256]{1,0:T(8,128)(2,1)} %key_ref.1, ...), custom_call_target="tpu_custom_call" | custom-call | tf_op jit(solution)/shard_map/attention_grads/pallas_call | solution.py:397
  63.3 0.0 copy-start.2
  63.3 0.0 copy-done
  63.4 1.7 %fusion.1 = f32[512,2048]{1,0:T(8,128)S(1)} fusion(bf16[2048,256]{1,0:T(8,128)(2,1)S(1)} %copy-done, bf16[512,512]{1,0:T(8,128)(2,1)} %get-tuple-element.7), kind=kOutput, calls=%fused_computation.2 | convolution fusion | flops 536870912 | bytes 5505024 | tf_op jit(solution)/shard_map/dot_general | solution.py:21
  65.1 0.0 copy-done.1
  65.1 0.0 copy-done.2
  65.1 0.0 copy-start.3
  65.1 0.0 copy-start.4
  65.1 2.8 %convolution_add_fusion = f32[512,2048]{1,0:T(8,128)} fusion(f32[512,2048]{1,0:T(8,128)S(1)} %fusion.1, bf16[2048,256]{1,0:T(8,128)(2,1)S(1)} %copy-done.1, bf16[512,512]{1,0:T(8,128)(2,1)S(1)} %copy-done.2), kind=kOutput, calls=%fused_computation | convolution fusion | flops 537919488 | bytes 9699328 | tf_op jit(solution)/shard_map/dot_general | solution.py:21
  67.9 0.0 copy-done.3
  67.9 0.7 %copy.14 = f32[128,512]{1,0:T(8,128)} copy(f32[128,512]{1,0:T(8,128)S(1)} %copy-done.3) | data formatting | bytes 524288
  68.6 0.0 copy-done.4
  68.6 0.7 copy.15
Async XLA Ops:
  0.6 62.7 %copy-start = (bf16[2048,256]{1,0:T(8,128)(2,1)S(1)}, bf16[2048,256]{1,0:T(8,128)(2,1)}, u32[]{:S(2)}) copy-start(bf16[2048,256]{1,0:T(8,128)(2,1)} %param.16) | copy-start | bytes 3145732
  0.6 64.5 %copy-start.1 = (bf16[2048,256]{1,0:T(8,128)(2,1)S(1)}, bf16[2048,256]{1,0:T(8,128)(2,1)}, u32[]{:S(2)}) copy-start(bf16[2048,256]{1,0:T(8,128)(2,1)} %param.17) | copy-start | bytes 3145732
  63.3 1.8 %copy-start.2 = (bf16[512,512]{1,0:T(8,128)(2,1)S(1)}, bf16[512,512]{1,0:T(8,128)(2,1)}, u32[]{:S(2)}) copy-start(bf16[512,512]{1,0:T(8,128)(2,1)} %get-tuple-element.7) | copy-start | bytes 1572868
  65.1 2.8 %copy-start.3 = (f32[128,512]{1,0:T(8,128)S(1)}, f32[128,512]{1,0:T(8,128)}, u32[]{:S(2)}) copy-start(f32[128,512]{1,0:T(8,128)} %get-tuple-element.12) | copy-start | bytes 786436
  65.1 3.5 %copy-start.4 = (f32[16,2048]{1,0:T(8,128)S(1)}, f32[16,2048]{1,0:T(8,128)}, u32[]{:S(2)}) copy-start(f32[16,2048]{1,0:T(8,128)} %get-tuple-element.14) | copy-start | bytes 393220
where the time goes:
time: 69.4 us; the launch traced here: 69.3 us
  Pallas kernels  62.7 us (90%)
  matrix products  4.52 us (7%)
  local copies, waits for them, and re-layouts  1.38 us (2%)
  between operations  0.71 us (1%)
    pallas_call x1, Pallas kernels, shards(): pl.pallas_call(functools.partial(kernel, tgt_n, src_n, key_n, tp_n, src_r...  62.7 us
    dot_general x2, matrix products, dot_nt(): lax.dot_general(left, right, (((1,), (1,)), ((), ())), preferred_element_...  4.52 us

commit v1 on v0

v1 whole, which is shorter than its diff:
```python
import functools
import math

import jax
import jax.numpy as jnp
from jax import lax
from jax.experimental import pallas as pl
from jax.experimental.pallas import tpu as pltpu
from jax.sharding import PartitionSpec as P

HEADS = 8
KV_HEADS = 2
HEAD_DIM = 128
HALVES = 2
LOG2E = 1.0 / math.log(2.0)
MESH = pl.DeviceIdType.MESH
F32 = jnp.float32
BF16 = jnp.bfloat16
VMEM_BYTES = 67_043_328


def dot_nt(left, right, precision=None):
    return lax.dot_general(
        left, right, (((1,), (1,)), ((), ())), preferred_element_type=F32, precision=precision
    )


def dot_tn(left, right):
    return lax.dot_general(left, right, (((0,), (0,)), ((), ())), preferred_element_type=F32)


def dot_nn(left, right):
    return jnp.dot(left, right, preferred_element_type=F32)


def kernel(
    tgt_n, src_n, key_n, tp_n, src_total,
    q_hbm, o_hbm, d_hbm, lse_hbm, key_hbm, value_hbm, source_hbm, kw_hbm, vw_hbm,
    dq_ref, sg_ref, kg_ref,
    kv_ref, weights,    o_own, lse_own, qd, stats, kvs, dk, dv, dq_acc, dq_out, dq_in, dq_via, g_out, g_in, g_via, tp_own, tp_in,
    src, a_out, a_in, a2_own, a2_out, a2_in, b_out, b_in, b2_own, b2_out, b2_in,
    copy_sem, load_kv, load_q, load_o, qd_s, qd_r, rq_s, st_s, st_r, kv_s, kv_r, rkv_s, dq_s, dq_r, via_r, g_s, g_r, gv_s, gv_r, tp_s, tp_r,
    a_s, a_r, a2_s, a2_r, b_s, b_r, b2_s, b2_r,
):
    sp = lax.axis_index("sp")
    tp = lax.axis_index("tp")
    sp_n = tgt_n * src_n
    t_hi, t_lo = sp // (2 * src_n), sp % 2
    me_t = t_hi * 2 + t_lo
    me_s = (sp // 2) % src_n
    s_hi, s_lo = me_s // 2, me_s % 2
    near_t, near_s = t_hi * 2 + 1 - t_lo, s_hi * 2 + 1 - s_lo
    t_his = [lax.rem(t_hi + k, tgt_n // 2) for k in range(1, tgt_n // 2)]
    s_his = [lax.rem(s_hi + k, src_n // 2) for k in range(1, src_n // 2)]
    far_t = [hi * 2 + t_lo for hi in t_his]
    diag_t = [hi * 2 + 1 - t_lo for hi in t_his]
    far_s = [hi * 2 + s_lo for hi in s_his]
    diag_s = [hi * 2 + 1 - s_lo for hi in s_his]
    t_peers = far_t + [near_t] + diag_t
    s_peers = far_s + [near_s] + diag_s
    key_m = sp_n // key_n
    me_o, me_i = sp // key_n, sp % key_n
    o_peers = [lax.rem(me_o + k, key_m) for k in range(1, key_m)]
    i_peers = [lax.rem(me_i + k, key_n) for k in range(1, key_n)]
    tp_peers = [lax.rem(tp + k, tp_n) for k in range(1, tp_n)]
    rows = q_hbm.shape[0]
    heads = q_hbm.shape[1] // HEAD_DIM
    chunks = stats.shape[1]
    src_rows = dk.shape[1]
    split = (chunks + 1) // 2
    per_chunk = heads // chunks
    per_key = HEADS // KV_HEADS
    scale = 1.0 / math.sqrt(HEAD_DIM)
    kv_col = pl.multiple_of(tp * heads // per_key * HEAD_DIM, HEAD_DIM)

    def t_dev(t):
        return {"sp": t // 2 * (2 * src_n) + me_s * 2 + t % 2, "tp": tp}

    def s_dev(s):
        return {"sp": t_hi * (2 * src_n) + s * 2 + t_lo, "tp": tp}

    def o_dev(o):
        return {"sp": o * key_n + me_i, "tp": tp}

    def i_dev(i):
        return {"sp": me_o * key_n + i, "tp": tp}

    def tp_dev(p):
        return {"sp": sp, "tp": p}

    def remote(source, target, send, recv, device):
        return pltpu.make_async_remote_copy(
            src_ref=source, dst_ref=target, send_sem=send, recv_sem=recv,
            device_id=device, device_id_type=MESH,
        )

    partners = (
        [t_dev(t) for t in t_peers] + [s_dev(s) for s in s_peers]
        + [o_dev(o) for o in o_peers] + [i_dev(i) for i in i_peers] + [tp_dev(p) for p in tp_peers]
    )
    barrier = pltpu.get_barrier_semaphore()
    for device in partners:
        pl.semaphore_signal(barrier, inc=1, device_id=device, device_id_type=MESH)
    piece = src_rows // HALVES
    chunk_w = per_chunk * HEAD_DIM
    loads = []
    for h in range(HALVES):
        for i, ref in enumerate((key_hbm, value_hbm)):
            loads.append(pltpu.make_async_copy(
                ref.at[pl.ds(h * piece, piece), pl.ds(kv_col, HEAD_DIM)],
                kvs.at[me_s, h, i], load_kv.at[2 * h + i],
            ))
    for c in range(chunks):
        for i, ref in enumerate((q_hbm, d_hbm)):
            loads.append(pltpu.make_async_copy(
                ref.at[:, pl.ds(c * chunk_w, chunk_w)], qd.at[me_t, c, i], load_q.at[c, i]
            ))
    loads.append(pltpu.make_async_copy(o_hbm, o_own, load_o.at[0]))
    loads.append(pltpu.make_async_copy(lse_hbm, lse_own, load_o.at[1]))
    lates = [pltpu.make_async_copy(source_hbm, src, copy_sem.at[0])]
    for i, ref in enumerate((kw_hbm, vw_hbm)):
        lates.append(pltpu.make_async_copy(ref, weights.at[i], copy_sem.at[1 + i]))
    for copy in loads:
        copy.start()
    for copy in lates:
        copy.start()
    dk[...] = jnp.zeros_like(dk)
    dv[...] = jnp.zeros_like(dv)
    dq_acc[...] = jnp.zeros_like(dq_acc)
    for copy in loads:
        copy.wait()
    ones = jnp.ones((8, HEAD_DIM), F32)
    for h in range(heads):
        cols = pl.ds(h * HEAD_DIM, HEAD_DIM)
        c, span = h // per_chunk, pl.ds(h % per_chunk * rows, rows)
        grad = qd[me_t, c, 1, :, pl.ds(h % per_chunk * HEAD_DIM, HEAD_DIM)]
        prod = grad.astype(F32) * o_own[:, cols].astype(F32)
        delta = dot_nt(ones, prod, lax.Precision.HIGHEST)
        stats[me_t, c, 0:1, span] = lse_own[h : h + 1, :] * LOG2E
        stats[me_t, c, 1:2, span] = delta[0:1, :]
    pl.semaphore_wait(barrier, len(partners))

    def send_q(t, c):
        return remote(
            qd.at[me_t, c], qd.at[me_t, c], qd_s.at[t, c], qd_r.at[me_t, c], t_dev(t)
        )

    def send_kv(s, h):
        return remote(
            kvs.at[me_s, h], kvs.at[me_s, h], kv_s.at[s, h], kv_r.at[me_s, h], s_dev(s)
        )

    for n in range(max(HALVES, chunks)):
        if n < HALVES:
            for s in far_s + [near_s]:
                send_kv(s, n).start()
        if n < chunks:
            for t in far_t + [near_t]:
                send_q(t, n).start()
        if n == 0:
            for t in t_peers:
                remote(
                    stats.at[me_t], stats.at[me_t], st_s.at[t], st_r.at[me_t], t_dev(t)
                ).start()

    def stack(t, i, c):
        return jnp.concatenate(
            [qd[t, c, i, :, h * HEAD_DIM : (h + 1) * HEAD_DIM] for h in range(per_chunk)], axis=0
        )

    def tile(t, s, low=0, high=chunks):
        def body(c, carry):
            q, d = stack(t, 0, c), stack(t, 1, c)
            k = kvs[s, :, 0].reshape(src_rows, HEAD_DIM)
            v = kvs[s, :, 1].reshape(src_rows, HEAD_DIM)
            scores = dot_nt(k, q)
            probs = jnp.exp2(scores * (scale * LOG2E) - stats[t, c, 0:1, :])
            dprobs = dot_nt(v, d)
            dscores = (probs * (dprobs - stats[t, c, 1:2, :])).astype(BF16)
            dv[s] += dot_nn(probs.astype(BF16), d)
            dk[s] += dot_nn(dscores, q)
            dq_acc[t, c] += dot_tn(dscores, k)
            return carry

        if low < high:
            lax.fori_loop(low, high, body, 0)

    def got_q(t, c):
        remote(qd.at[t, c], qd.at[t, c], qd_s.at[t, c], qd_r.at[t, c], t_dev(t)).wait_recv()

    def got_stats(t):
        remote(stats.at[t], stats.at[t], st_s.at[t], st_r.at[t], t_dev(t)).wait_recv()

    def got_kv(s, h):
        remote(kvs.at[s, h], kvs.at[s, h], kv_s.at[s, h], kv_r.at[s, h], s_dev(s)).wait_recv()

    def relay_q(t, c):
        return remote(
            qd.at[t, c], qd.at[t, c], rq_s.at[t, c], qd_r.at[t, c], t_dev(near_t)
        )

    def relay_kv(s, h):
        return remote(
            kvs.at[s, h], kvs.at[s, h], rkv_s.at[s, h], kv_r.at[s, h], s_dev(near_s)
        )

    def pass_q(low, high):
        for c in range(low, high):
            for t in far_t:
                got_q(t, c)
                relay_q(t, c).start()

    def pass_kv(h):
        for s in far_s:
            got_kv(s, h)
            relay_kv(s, h).start()

    def dq_copy(t):
        return remote(dq_out.at[t], dq_in.at[me_t], dq_s.at[t], dq_r.at[me_t], t_dev(t))

    def g_term(s, i):
        return dv[s] if i else dk[s] * scale

    def g_copy(s, i):
        return remote(
            g_out.at[s, i], g_in.at[me_s, i], g_s.at[s, i], g_r.at[me_s, i], s_dev(s)
        )

    def via_copy(n, i):
        return remote(
            g_out.at[diag_s[n], i], g_via.at[me_s, i], gv_s.at[far_s[n], i],
            gv_r.at[me_s, i], s_dev(far_s[n]),
        )

    def send_via(i):
        for n, s in enumerate(diag_s):
            g_out[s, i] = g_term(s, i).astype(BF16)
            via_copy(n, i).start()

    def send_far(i):
        for s in far_s:
            g_out[s, i] = g_term(s, i).astype(BF16)
            g_copy(s, i).start()

    def send_near(i):
        total = g_term(near_s, i)
        for s in far_s:
            remote(
                g_via.at[s, i], g_via.at[s, i], gv_s.at[s, i], gv_r.at[s, i], s_dev(s)
            ).wait_recv()
            total += g_via[s, i].astype(F32)
        g_out[near_s, i] = total.astype(BF16)
        g_copy(near_s, i).start()

    tile(me_t, me_s)
    got_stats(near_t)
    for c in range(chunks):
        got_q(near_t, c)
        tile(near_t, me_s, c, c + 1)
    pass_kv(0)
    for h in range(HALVES):
        got_kv(near_s, h)
    tile(me_t, near_s)
    pass_q(0, split)
    tile(near_t, near_s)
    for t in far_t:
        got_stats(t)
        for s in [me_s, near_s]:
            tile(t, s, 0, split)
    for h in range(1, HALVES):
        pass_kv(h)
    pass_q(split, chunks)
    for s in far_s:
        for t in [me_t, near_t]:
            tile(t, s)
    for t in far_t:
        for s in [me_s, near_s]:
            tile(t, s, split, chunks)
    for s in diag_s:
        for h in range(HALVES):
            got_kv(s, h)
        for t in [near_t, me_t] + far_t:
            tile(t, s)
    dq_out[near_t] = (dq_acc[near_t] * scale).astype(BF16)
    dq_copy(near_t).start()
    for t in diag_t:
        got_stats(t)
        for c in range(chunks):
            got_q(t, c)
        for s in diag_s:
            tile(t, s)
    send_via(0)
    for s in far_s:
        for t in far_t + diag_t:
            tile(t, s)
    send_far(0)
    for t in diag_t:
        for s in [near_s, me_s]:
            tile(t, s)
    send_near(0)
    for t in diag_t:
        dq_out[t] = (dq_acc[t] * scale).astype(BF16)
        remote(dq_out.at[t], dq_via.at[t], dq_s.at[t], via_r.at[t], t_dev(near_t)).start()
    send_via(1)
    send_far(1)

    def reduce_g(i):
        total = g_term(me_s, i)
        for s in far_s + [near_s]:
            remote(
                g_in.at[s, i], g_in.at[s, i], g_s.at[s, i], g_r.at[s, i], s_dev(s)
            ).wait_recv()
            total += g_in[s, i].astype(F32)
        tp_own[i] = total.astype(BF16)
        for p in tp_peers:
            remote(
                tp_own.at[i], tp_in.at[tp, i], tp_s.at[p, i], tp_r.at[tp, i], tp_dev(p)
            ).start()
        tp_in[tp, i] = tp_own[i]

    def gather_g(i):
        for p in tp_peers:
            remote(
                tp_in.at[p, i], tp_in.at[p, i], tp_s.at[p, i], tp_r.at[p, i], tp_dev(p)
            ).wait_recv()
        for g in range(KV_HEADS):
            owners = [p for p in range(tp_n) if p * heads // per_key == g]
            half = tp_in[owners[0], i]
            if len(owners) > 1:
                total = half.astype(F32)
                for p in owners[1:]:
                    total += tp_in[p, i].astype(F32)
                half = total.astype(BF16)
            kv_ref[:, pl.ds((i * KV_HEADS + g) * HEAD_DIM, HEAD_DIM)] = half

    reduce_g(0)
    lates[0].wait()
    gather_g(0)
    part = a2_own.shape[1]
    cut = a2_own.shape[2]
    key_half = kv_ref[:, 0 : KV_HEADS * HEAD_DIM]
    w_scale = 1.0 / math.sqrt(src_total)
    partial = dot_tn(key_half, src[...]) * w_scale
    for o in range(key_m):
        for i in range(key_n):
            low = (o * key_n + i) * part
            block = partial[low : low + part].astype(BF16)
            a_out[i, o] = block[:, :cut]
            b_out[o, i] = block[:, cut:]
    for i in i_peers:
        remote(a_out.at[i], a_in.at[me_i], a_s.at[i], a_r.at[me_i], i_dev(i)).start()
    for o in o_peers:
        remote(b_out.at[o], b_in.at[me_o], b_s.at[o], b_r.at[me_o], o_dev(o)).start()

    send_near(1)
    for t in far_t:
        remote(dq_out.at[t], dq_via.at[t], dq_s.at[t], via_r.at[t], t_dev(near_t)).wait_recv()
        dq_out[t] = (dq_acc[t] * scale + dq_via[t].astype(F32)).astype(BF16)
        dq_copy(t).start()

    total = b_out[me_o].astype(F32)
    for o in o_peers:
        remote(b_in.at[o], b_in.at[o], b_s.at[o], b_r.at[o], o_dev(o)).wait_recv()
        total += b_in[o].astype(F32)
    b2_own[...] = total
    b2_out[...] = total.astype(BF16)
    for i in i_peers:
        remote(b2_out.at[i], b2_in.at[me_i], b2_s.at[i], b2_r.at[me_i], i_dev(i)).start()
    total = a_out[me_i].astype(F32)
    for i in i_peers:
        remote(a_in.at[i], a_in.at[i], a_s.at[i], a_r.at[i], i_dev(i)).wait_recv()
        total += a_in[i].astype(F32)
    a2_own[...] = total
    a2_out[...] = total.astype(BF16)
    for o in o_peers:
        remote(a2_out.at[o], a2_in.at[me_o], a2_s.at[o], a2_r.at[me_o], o_dev(o)).start()
    reduce_g(1)
    gather_g(1)
    for copy in lates[1:]:
        copy.wait()
    kv_width = KV_HEADS * HEAD_DIM
    span = sg_ref.shape[1] // 4

    def source_tile(n, carry):
        cols = pl.ds(pl.multiple_of(n * span, HEAD_DIM), span)
        sg_ref[:, cols] = dot_nt(kv_ref[:, :kv_width], weights[0, cols, :]) + dot_nt(
            kv_ref[:, kv_width:], weights[1, cols, :]
        )
        return carry

    lax.fori_loop(0, 4, source_tile, 0)
    dq_total = dq_acc[me_t] * scale
    for t in [near_t] + far_t:
        remote(dq_in.at[t], dq_in.at[t], dq_s.at[t], dq_r.at[t], t_dev(t)).wait_recv()
        dq_total += dq_in[t].astype(F32)
    for h in range(heads):
        low = h % per_chunk * rows
        dq_ref[:, h * HEAD_DIM : (h + 1) * HEAD_DIM] = dq_total[h // per_chunk, low : low + rows]

    total = b2_own[me_i]
    for i in i_peers:
        remote(b2_in.at[i], b2_in.at[i], b2_s.at[i], b2_r.at[i], i_dev(i)).wait_recv()
        total += b2_in[i].astype(F32)
    kg_ref[:, cut:] = total
    total = a2_own[me_o]
    for o in o_peers:
        remote(a2_in.at[o], a2_in.at[o], a2_s.at[o], a2_r.at[o], o_dev(o)).wait_recv()
        total += a2_in[o].astype(F32)
    kg_ref[:, :cut] = total

    for c in range(chunks):
        for t in far_t + [near_t]:
            send_q(t, c).wait_send()
        for t in far_t:
            relay_q(t, c).wait_send()
    for h in range(HALVES):
        for s in far_s + [near_s]:
            send_kv(s, h).wait_send()
        for s in far_s:
            relay_kv(s, h).wait_send()
    for t in t_peers:
        remote(stats.at[t], stats.at[t], st_s.at[t], st_r.at[t], t_dev(t)).wait_send()
        remote(dq_out.at[t], dq_in.at[t], dq_s.at[t], dq_r.at[t], t_dev(t)).wait_send()
    for i in range(2):
        for s in far_s + [near_s]:
            g_copy(s, i).wait_send()
        for n in range(len(diag_s)):
            via_copy(n, i).wait_send()
    for i in i_peers:
        remote(a_out.at[i], a_in.at[i], a_s.at[i], a_r.at[i], i_dev(i)).wait_send()
        remote(b2_out.at[i], b2_in.at[i], b2_s.at[i], b2_r.at[i], i_dev(i)).wait_send()
    for o in o_peers:
        remote(b_out.at[o], b_in.at[o], b_s.at[o], b_r.at[o], o_dev(o)).wait_send()
        remote(a2_out.at[o], a2_in.at[o], a2_s.at[o], a2_r.at[o], o_dev(o)).wait_send()
    for p in tp_peers:
        for i in range(2):
            remote(
                tp_own.at[i], tp_in.at[p, i], tp_s.at[p, i], tp_r.at[p, i], tp_dev(p)
            ).wait_send()


def finish(*refs):
    *refs, sem = refs
    copies = [
        pltpu.make_async_copy(value, out, sem.at[n])
        for n, (value, out) in enumerate(zip(refs[:3], refs[3:]))
    ]
    for copy in copies:
        copy.start()
    for copy in copies:
        copy.wait()


def shards(
    tgt_n, src_n, tp_n,
    queries, attn_out, out_grad, row_lse, source, saved_keys, saved_values, key_weight, value_weight
):
    heads = row_lse.shape[1]
    rows, width = queries.shape
    src_rows, columns = source.shape
    kv_width = KV_HEADS * HEAD_DIM
    sp_n = tgt_n * src_n
    part = kv_width // sp_n
    key_n, key_m = src_n, tgt_n
    chunks = math.gcd(heads, 2)
    stacked = heads // chunks * rows
    cut = (2 * columns // 3 + 127) // 128 * 128
    rest = columns - cut
    dma = pltpu.SemaphoreType.DMA
    vmem = pl.BlockSpec(memory_space=pltpu.VMEM)
    hbm = pl.BlockSpec(memory_space=pltpu.HBM)
    scratch = [
        pltpu.VMEM((src_rows, 2 * kv_width), BF16),
        pltpu.VMEM((2, columns, kv_width), BF16),
        pltpu.VMEM((rows, width), BF16),
        pltpu.VMEM((heads, rows), F32),
        pltpu.VMEM((tgt_n, chunks, 2, rows, width // chunks), BF16),
        pltpu.VMEM((tgt_n, chunks, 8, stacked), F32),
        pltpu.VMEM((src_n, HALVES, 2, src_rows // HALVES, HEAD_DIM), BF16),
        pltpu.VMEM((src_n, src_rows, HEAD_DIM), F32),
        pltpu.VMEM((src_n, src_rows, HEAD_DIM), F32),
        pltpu.VMEM((tgt_n, chunks, stacked, HEAD_DIM), F32),
        pltpu.VMEM((tgt_n, chunks, stacked, HEAD_DIM), BF16),
        pltpu.VMEM((tgt_n, chunks, stacked, HEAD_DIM), BF16),
        pltpu.VMEM((tgt_n, chunks, stacked, HEAD_DIM), BF16),
        pltpu.VMEM((src_n, 2, src_rows, HEAD_DIM), BF16),
        pltpu.VMEM((src_n, 2, src_rows, HEAD_DIM), BF16),
        pltpu.VMEM((src_n, 2, src_rows, HEAD_DIM), BF16),
        pltpu.VMEM((2, src_rows, HEAD_DIM), BF16),
        pltpu.VMEM((tp_n, 2, src_rows, HEAD_DIM), BF16),
        pltpu.VMEM((src_rows, columns), BF16),
        pltpu.VMEM((key_n, key_m, part, cut), BF16),
        pltpu.VMEM((key_n, key_m, part, cut), BF16),
        pltpu.VMEM((key_m, part, cut), F32),
        pltpu.VMEM((key_m, part, cut), BF16),
        pltpu.VMEM((key_m, part, cut), BF16),
        pltpu.VMEM((key_m, key_n, part, rest), BF16),
        pltpu.VMEM((key_m, key_n, part, rest), BF16),
        pltpu.VMEM((key_n, part, rest), F32),
        pltpu.VMEM((key_n, part, rest), BF16),
        pltpu.VMEM((key_n, part, rest), BF16),
        dma((3,)),
        dma((2 * HALVES,)),
        dma((chunks, 2)),
        dma((2,)),
    ]
    for shape in (
        (tgt_n, chunks), (tgt_n, chunks), (tgt_n, chunks), (tgt_n,), (tgt_n,),
        (src_n, HALVES), (src_n, HALVES), (src_n, HALVES), (tgt_n,), (tgt_n,), (tgt_n,),
        (src_n, 2), (src_n, 2), (src_n, 2), (src_n, 2),
        (tp_n, 2), (tp_n, 2), (key_n,), (key_n,), (key_m,), (key_m,),
        (key_m,), (key_m,), (key_n,), (key_n,),
    ):
        scratch.append(dma(shape))
    shapes = ((rows, width), (src_rows, columns), (part, columns))
    grads = pl.pallas_call(
        functools.partial(kernel, tgt_n, src_n, key_n, tp_n, src_rows * sp_n),
        out_shape=[pltpu.VMEM(shape, F32) for shape in shapes],
        in_specs=[hbm] * 9,
        out_specs=[vmem] * 3,
        scratch_shapes=scratch,
        compiler_params=pltpu.CompilerParams(
            collective_id=0, has_side_effects=True,
            vmem_limit_bytes=VMEM_BYTES - 4 * sum(map(math.prod, shapes)),
        ),
        name="attention_grads",
    )(
        queries, attn_out, out_grad, row_lse.T, saved_keys, saved_values, source,
        key_weight, value_weight,
    )
    return tuple(pl.pallas_call(
        finish,
        out_shape=[jax.ShapeDtypeStruct(shape, F32) for shape in shapes],
        in_specs=[vmem] * 3,
        out_specs=[hbm] * 3,
        scratch_shapes=[dma((3,))],
        compiler_params=pltpu.CompilerParams(vmem_limit_bytes=2**20),
        name="write_grads",
    )(*grads))


def solution(mesh):
    sp_n, tp_n = mesh.shape["sp"], mesh.shape["tp"]
    src_n = 2 ** (int(math.log2(sp_n)) // 2)
    in_specs = (
        P("sp", "tp"),
        P("sp", "tp"),
        P("sp", "tp"),
        P("sp", "tp"),
        P("sp", "tp"),
        P("sp", None),
        P("sp", None),
        P("tp", None),
        P("tp", None),
    )
    out_specs = (P("sp", "tp"), P("sp", "tp"), P("sp", "tp"))
    return jax.shard_map(
        functools.partial(shards, sp_n // src_n, src_n, tp_n),
        mesh=mesh, in_specs=in_specs, out_specs=out_specs, check_vma=False,
    )
```

time: 69.4 us -> 61.3 us (0.88)
  matrix products: 4.52 us -> 0 us
  Pallas kernels: 62.7 us -> 60.6 us
  local copies, waits for them, and re-layouts: 1.38 us -> 0 us
    dot_general x2 -> x0, matrix products: 4.52 us -> none  [dot_nt(): lax.dot_general(left, right, (((1,), (1,)), ((), ())), preferred_element_...]
    pallas_call x1, Pallas kernels: 62.7 us -> 58.4 us  [shards(): pl.pallas_call(functools.partial(kernel, tgt_n, src_n, key_n, tp_n, src_r...]
    pallas_call x0 -> x1, Pallas kernels: none -> 2.15 us  [shards(): pl.pallas_call(finish, out_shape=[jax.ShapeDtypeStruct(shape, F32) for sh...]
    unnamed x12 -> x0, local copies, waits for them, and re-layouts: 1.38 us -> none
where the time goes in v1:
time: 61.3 us; the launch traced here: 61.2 us
  Pallas kernels  60.6 us (99%)
  between operations  0.64 us (1%)
    pallas_call x1, Pallas kernels, shards(): pl.pallas_call(functools.partial(kernel, tgt_n, src_n, key_n, tp_n, src_r...  58.4 us
    pallas_call x1, Pallas kernels, shards(): pl.pallas_call(finish, out_shape=[jax.ShapeDtypeStruct(shape, F32) for sh...  2.15 us

profile of v1, /device:TPU:0, one launch (start us, length us, event | category | flops | bytes accessed | tf_op | source)
XLA Modules:
  0.0 61.2 jit_solution(1113152045772658451)
XLA Ops:
  0.6 58.4 %attention_grads.1 = (f32[128,512]{1,0:T(8,128)S(1)}, f32[512,2048]{1,0:T(8,128)S(1)}, f32[16,2048]{1,0:T(8,128)S(1)}) custom-call(bf16[128,512]{1,0:T(8,128)(2,1)} %q_hbm.1, bf16[128,512]{1,0:T(8,128)(2,1)} %o_hbm.1, bf16[128,512]{1,0:T(8,128)(2,1)} %d_hbm.1, f32[4,128]{1,0:T(4,128)} %bitcast.1, bf16[512,256]{1,0:T(8,128)(2,1)} %key_hbm.1, ...), custom_call_target="tpu_custom_call" | custom-call | tf_op jit(solution)/shard_map/attention_grads/pallas_call | solution.py:516
  59.0 2.1 %write_grads.1 = (f32[128,512]{1,0:T(8,128)}, f32[512,2048]{1,0:T(8,128)}, f32[16,2048]{1,0:T(8,128)}) custom-call(f32[128,512]{1,0:T(8,128)S(1)} %get-tuple-element.6.refs_0_, f32[512,2048]{1,0:T(8,128)S(1)} %get-tuple-element.7.refs_1_, f32[16,2048]{1,0:T(8,128)S(1)} %get-tuple-element.8.refs_2_), custom_call_target="tpu_custom_call" | custom-call | tf_op jit(solution)/shard_map/write_grads/pallas_call | solution.py:531

commit v2 on v1

v2 whole, which is shorter than its diff:
```python
import functools
import math

import jax
import jax.numpy as jnp
from jax import lax
from jax.experimental import pallas as pl
from jax.experimental.pallas import tpu as pltpu
from jax.sharding import PartitionSpec as P

HEADS = 8
KV_HEADS = 2
HEAD_DIM = 128
HALVES = 2
PIECES = 3
LOG2E = 1.0 / math.log(2.0)
MESH = pl.DeviceIdType.MESH
F32 = jnp.float32
BF16 = jnp.bfloat16
VMEM_BYTES = 67_043_328


def dot_nt(left, right, precision=None):
    return lax.dot_general(
        left, right, (((1,), (1,)), ((), ())), preferred_element_type=F32, precision=precision
    )


def dot_tn(left, right):
    return lax.dot_general(left, right, (((0,), (0,)), ((), ())), preferred_element_type=F32)


def dot_nn(left, right):
    return jnp.dot(left, right, preferred_element_type=F32)


def kernel(
    tgt_n, src_n, key_n, tp_n, src_total,
    q_hbm, o_hbm, d_hbm, lse_hbm, key_hbm, value_hbm, source_hbm, kw_hbm, vw_hbm,
    dq_ref, sg_ref, kg_ref,
    kv_ref, weights,    o_own, lse_own, qd, stats, kvs, dk, dv, dq_acc, dq_out, dq_in, d_out, g_via, g_out, g_in, tp_own, tp_in,
    src, a_out, a_in, a2_own, a2_out, a2_in, b_out, b_in, b2_own, b2_out, b2_in,
    copy_sem, load_kv, load_q, load_o, up_s, down_s, qd_r, st_s, st_r, kvx_s, kvy_s, kv_r, rkv_s, dq_s, dq_r, via_s, via_r, g_s, g_r, tp_s, tp_r,
    a_s, a_r, a2_s, a2_r, b_s, b_r, b2_s, b2_r,
):
    sp = lax.axis_index("sp")
    tp = lax.axis_index("tp")
    sp_n = tgt_n * src_n
    me_t, me_s = sp // src_n, sp % src_n
    x_s = me_s + 1 - 2 * (me_s % 2)
    y_s, d_s = (me_s + 2) % src_n, (x_s + 2) % src_n
    s_peers = [d_s, x_s, y_s]
    t_peers = [lax.rem(me_t + k, tgt_n) for k in range(1, tgt_n)]
    below, above = me_t, tgt_n - 1 - me_t
    paired = jnp.minimum(below, above)
    longer = jnp.where(above > below, 1, -1)
    inner = paired > 0
    order = []
    for j in range(tgt_n - 1):
        both = me_t + (j // 2 + 1) * (1 if j % 2 == 0 else -1)
        order.append(jnp.where(j < 2 * paired, both, me_t + longer * (j - paired + 1)))
    key_m = tgt_n
    me_o, me_i = me_t, me_s
    o_peers, i_peers = t_peers, s_peers
    tp_peers = [lax.rem(tp + k, tp_n) for k in range(1, tp_n)]
    rows = q_hbm.shape[0]
    heads = q_hbm.shape[1] // HEAD_DIM
    chunks = qd.shape[1]
    src_rows = dk.shape[1]
    stacked = stats.shape[2]
    split = (chunks + 1) // 2
    per_chunk = heads // chunks
    per_key = HEADS // KV_HEADS
    scale = 1.0 / math.sqrt(HEAD_DIM)
    kv_col = pl.multiple_of(tp * heads // per_key * HEAD_DIM, HEAD_DIM)

    def t_dev(t):
        return {"sp": t * src_n + me_s, "tp": tp}

    def s_dev(s):
        return {"sp": me_t * src_n + s, "tp": tp}

    o_dev, i_dev = t_dev, s_dev

    def tp_dev(p):
        return {"sp": sp, "tp": p}

    def remote(source, target, send, recv, device):
        return pltpu.make_async_remote_copy(
            src_ref=source, dst_ref=target, send_sem=send, recv_sem=recv,
            device_id=device, device_id_type=MESH,
        )

    partners = (
        [t_dev(t) for t in t_peers] + [s_dev(s) for s in s_peers] + [tp_dev(p) for p in tp_peers]
    )
    barrier = pltpu.get_barrier_semaphore()
    for device in partners:
        pl.semaphore_signal(barrier, inc=1, device_id=device, device_id_type=MESH)
    piece = src_rows // HALVES
    chunk_w = per_chunk * HEAD_DIM
    loads = []
    for h in range(HALVES):
        for i, ref in enumerate((key_hbm, value_hbm)):
            loads.append(pltpu.make_async_copy(
                ref.at[pl.ds(h * piece, piece), pl.ds(kv_col, HEAD_DIM)],
                kvs.at[me_s, h, i], load_kv.at[2 * h + i],
            ))
    for c in range(chunks):
        for i, ref in enumerate((q_hbm, d_hbm)):
            loads.append(pltpu.make_async_copy(
                ref.at[:, pl.ds(c * chunk_w, chunk_w)], qd.at[me_t, c, i], load_q.at[c, i]
            ))
    loads.append(pltpu.make_async_copy(o_hbm, o_own, load_o.at[0]))
    loads.append(pltpu.make_async_copy(lse_hbm, lse_own, load_o.at[1]))
    lates = [pltpu.make_async_copy(source_hbm, src, copy_sem.at[0])]
    for i, ref in enumerate((kw_hbm, vw_hbm)):
        lates.append(pltpu.make_async_copy(ref, weights.at[i], copy_sem.at[1 + i]))
    for copy in loads:
        copy.start()
    dk[...] = jnp.zeros_like(dk)
    dv[...] = jnp.zeros_like(dv)
    dq_acc[...] = jnp.zeros_like(dq_acc)
    for copy in loads:
        copy.wait()
    ones = jnp.ones((8, HEAD_DIM), F32)
    for h in range(heads):
        cols = pl.ds(h * HEAD_DIM, HEAD_DIM)
        c, span = h // per_chunk, pl.ds(h % per_chunk * rows, rows)
        grad = qd[me_t, c, 1, :, pl.ds(h % per_chunk * HEAD_DIM, HEAD_DIM)]
        prod = grad.astype(F32) * o_own[:, cols].astype(F32)
        delta = dot_nt(ones, prod, lax.Precision.HIGHEST)
        stats[me_t, 2 * c : 2 * c + 1, span] = lse_own[h : h + 1, :] * LOG2E
        stats[me_t, 2 * c + 1 : 2 * c + 2, span] = delta[0:1, :]
    pl.semaphore_wait(barrier, len(partners))
    for copy in lates:
        copy.start()

    def q_copy(block, t, c, sems):
        return remote(
            qd.at[block, c], qd.at[block, c], sems.at[block, c], qd_r.at[block, c], t_dev(t)
        )

    def kv_copy(block, s, h, sems):
        return remote(
            kvs.at[block, h], kvs.at[block, h], sems.at[h], kv_r.at[block, h], s_dev(s)
        )

    def stat_copy(t):
        return remote(stats.at[me_t], stats.at[me_t], st_s.at[t], st_r.at[me_t], t_dev(t))

    def on_line(act):
        @pl.when(above > 0)
        def _():
            act(me_t + 1, up_s)

        @pl.when(below > 0)
        def _():
            act(me_t - 1, down_s)

    for n in range(max(HALVES, chunks)):
        if n < HALVES:
            kv_copy(me_s, x_s, HALVES - 1 - n, kvx_s).start()
            kv_copy(me_s, y_s, n, kvy_s).start()
        if n < chunks:
            on_line(lambda t, sems, n=n: q_copy(me_t, t, n, sems).start())
        if n == 0:
            for t in t_peers:
                stat_copy(t).start()

    def stack(t, i, low, high):
        return jnp.concatenate(
            [
                qd[t, c, i, :, h * HEAD_DIM : (h + 1) * HEAD_DIM]
                for c in range(low, high) for h in range(per_chunk)
            ],
            axis=0,
        )

    def stat(t, i, low, high):
        return jnp.concatenate([stats[t, 2 * c + i : 2 * c + i + 1, :] for c in range(low, high)], axis=1)

    def keys(s, i):
        return kvs[s, :, i].reshape(src_rows, HEAD_DIM)

    def tile(t, s, low=0, high=chunks):
        if low == high:
            return
        q, d = stack(t, 0, low, high), stack(t, 1, low, high)
        k, v = keys(s, 0), keys(s, 1)
        scores = dot_nt(k, q)
        probs = jnp.exp2(scores * (scale * LOG2E) - stat(t, 0, low, high))
        dprobs = dot_nt(v, d)
        dscores = (probs * (dprobs - stat(t, 1, low, high))).astype(BF16)
        probs = probs.astype(BF16)
        dv[s] += dot_nn(probs, d)
        dk[s] += dot_nn(dscores, q)
        part_q = dot_tn(k, dscores)
        for c in range(low, high):
            span = (c - low) * stacked
            dq_acc[t, c] += part_q[:, span : span + stacked]

    def got_q(j, c):
        q_copy(order[j], me_t, c, up_s).wait_recv()

    def forward(j, c, act):
        @pl.when(order[j] > me_t)
        def _():
            act(q_copy(order[j], me_t - 1, c, down_s))

        @pl.when(order[j] < me_t)
        def _():
            act(q_copy(order[j], me_t + 1, c, up_s))

    def pass_q(j, c):
        @pl.when(inner)
        def _():
            got_q(j, c)
            forward(j, c, lambda copy: copy.start())

    def last_q(j, c):
        @pl.when(jnp.logical_not(inner))
        def _():
            got_q(j, c)

    def got_stats(t):
        remote(stats.at[t], stats.at[t], st_s.at[t], st_r.at[t], t_dev(t)).wait_recv()

    def got_kv(s, h):
        kv_copy(s, s, h, kvx_s).wait_recv()

    def dq_copy(t):
        return remote(dq_out.at[t], dq_in.at[me_t], dq_s.at[t], dq_r.at[me_t], t_dev(t))

    def g_part(s, i, h):
        span = pl.ds(h * piece, piece)
        return dv[s, span] if i else dk[s, span] * scale

    def via_copy(i, h):
        return remote(
            d_out.at[i, h], g_via.at[i, h], via_s.at[i, h], via_r.at[i, h], s_dev((x_s, y_s)[h])
        )

    def g_copy(i, n, h):
        return remote(
            g_out.at[i, n, h], g_in.at[i, n, h], g_s.at[i, n, h], g_r.at[i, n, h],
            s_dev((x_s, y_s)[n]),
        )

    def send_via(i):
        for h in range(HALVES):
            d_out[i, h] = g_part(d_s, i, h).astype(BF16)
            via_copy(i, h).start()

    def send_plain(i, n):
        g_out[i, n, n] = g_part((x_s, y_s)[n], i, n).astype(BF16)
        g_copy(i, n, n).start()

    def send_sum(i):
        for h in range(HALVES):
            n = 1 - h
            via_copy(i, h).wait_recv()
            total = g_part((x_s, y_s)[n], i, h) + g_via[i, h].astype(F32)
            g_out[i, n, h] = total.astype(BF16)
            g_copy(i, n, h).start()

    def send_dq(t):
        dq_out[t] = (dq_acc[t] * scale).astype(BF16)
        dq_copy(t).start()

    everyone = [me_s, x_s, y_s, d_s]
    tile(me_t, me_s)
    got_kv(y_s, 0)
    kv_copy(y_s, x_s, 0, rkv_s).start()
    for h in range(1, HALVES):
        got_kv(x_s, h)
        kv_copy(x_s, y_s, h, rkv_s).start()
    for c in range(split):
        pass_q(0, c)
        last_q(0, c)
        pass_q(1, c)
    got_stats(order[0])
    tile(order[0], me_s, 0, split)
    for h in range(1, HALVES):
        got_kv(y_s, h)
    got_kv(x_s, 0)
    for c in range(split, chunks):
        pass_q(0, c)
        last_q(0, c)
        pass_q(1, c)
    tile(order[0], me_s, split, chunks)
    for s in (x_s, y_s):
        tile(me_t, s)
    tile(order[0], x_s)
    for c in range(split):
        pass_q(2, c)
    for h in range(HALVES):
        got_kv(d_s, h)
    tile(order[0], y_s)
    for t in (me_t, order[0]):
        tile(t, d_s)
    send_dq(order[0])
    for c in range(split, chunks):
        pass_q(2, c)
    got_stats(order[1])
    for c in range(chunks):
        last_q(1, c)
    for s in everyone:
        tile(order[1], s)
    send_dq(order[1])
    for j in range(2, tgt_n - 1):
        got_stats(order[j])
        for c in range(chunks):
            if j > 2:
                pass_q(j, c)
            last_q(j, c)
            if c == split - 1:
                for s in everyone:
                    tile(order[j], s, 0, split)
        if j < tgt_n - 2:
            for s in everyone:
                tile(order[j], s, split, chunks)
            send_dq(order[j])
    for n, s in enumerate([d_s, x_s, y_s, me_s]):
        tile(order[-1], s, split, chunks)
        if n == 0:
            send_via(0)
        elif n < 3:
            send_plain(0, n - 1)
    send_dq(order[-1])
    send_sum(0)
    send_via(1)
    for n in range(2):
        send_plain(1, n)

    def reduce_g(i):
        for h in range(HALVES):
            total = g_part(me_s, i, h)
            for n in range(2):
                g_copy(i, n, h).wait_recv()
                total += g_in[i, n, h].astype(F32)
            tp_own[i, h * piece : (h + 1) * piece] = total.astype(BF16)
        for p in tp_peers:
            remote(
                tp_own.at[i], tp_in.at[tp, i], tp_s.at[p, i], tp_r.at[tp, i], tp_dev(p)
            ).start()
        tp_in[tp, i] = tp_own[i]

    def gather_g(i):
        for p in tp_peers:
            remote(
                tp_in.at[p, i], tp_in.at[p, i], tp_s.at[p, i], tp_r.at[p, i], tp_dev(p)
            ).wait_recv()
        for g in range(KV_HEADS):
            owners = [p for p in range(tp_n) if p * heads // per_key == g]
            half = tp_in[owners[0], i]
            if len(owners) > 1:
                total = half.astype(F32)
                for p in owners[1:]:
                    total += tp_in[p, i].astype(F32)
                half = total.astype(BF16)
            kv_ref[:, pl.ds((i * KV_HEADS + g) * HEAD_DIM, HEAD_DIM)] = half

    reduce_g(0)
    lates[0].wait()
    gather_g(0)
    pieces, part, cut = a2_own.shape[0], a2_own.shape[2], a2_own.shape[3]
    key_half = kv_ref[:, 0 : KV_HEADS * HEAD_DIM]
    w_scale = 1.0 / math.sqrt(src_total)

    def a_copy(p, i):
        return remote(
            a_out.at[p, i], a_in.at[p, me_i], a_s.at[p, i], a_r.at[p, me_i], i_dev(i)
        )

    def a2_copy(p, o):
        return remote(
            a2_out.at[p, o], a2_in.at[p, me_o], a2_s.at[p, o], a2_r.at[p, me_o], o_dev(o)
        )

    def a_part(p):
        partial = dot_tn(key_half, src[:, p * cut : (p + 1) * cut]) * w_scale
        for o in range(key_m):
            for i in range(key_n):
                low = (o * key_n + i) * part
                a_out[p, i, o] = partial[low : low + part].astype(BF16)
        for i in i_peers:
            a_copy(p, i).start()

    a_part(0)
    partial = dot_tn(key_half, src[:, pieces * cut :]) * w_scale
    for o in range(key_m):
        for i in range(key_n):
            low = (o * key_n + i) * part
            b_out[o, i] = partial[low : low + part].astype(BF16)
    for o in o_peers:
        remote(b_out.at[o], b_in.at[me_o], b_s.at[o], b_r.at[me_o], o_dev(o)).start()
    for p in range(1, pieces):
        a_part(p)
    send_sum(1)

    def a_sum(p):
        total = a_out[p, me_i].astype(F32)
        for i in i_peers:
            remote(
                a_in.at[p, i], a_in.at[p, i], a_s.at[p, i], a_r.at[p, i], i_dev(i)
            ).wait_recv()
            total += a_in[p, i].astype(F32)
        a2_own[p] = total
        a2_out[p] = total.astype(BF16)
        for o in o_peers:
            a2_copy(p, o).start()

    a_sum(0)
    total = b_out[me_o].astype(F32)
    for o in o_peers:
        remote(b_in.at[o], b_in.at[o], b_s.at[o], b_r.at[o], o_dev(o)).wait_recv()
        total += b_in[o].astype(F32)
    b2_own[...] = total
    b2_out[...] = total.astype(BF16)
    for i in i_peers:
        remote(b2_out.at[i], b2_in.at[me_i], b2_s.at[i], b2_r.at[me_i], i_dev(i)).start()
    for p in range(1, pieces):
        a_sum(p)

    reduce_g(1)
    gather_g(1)
    for copy in lates[1:]:
        copy.wait()
    kv_width = KV_HEADS * HEAD_DIM
    span = sg_ref.shape[1] // 4

    def source_tile(n, carry):
        cols = pl.ds(pl.multiple_of(n * span, HEAD_DIM), span)
        sg_ref[:, cols] = dot_nt(kv_ref[:, :kv_width], weights[0, cols, :]) + dot_nt(
            kv_ref[:, kv_width:], weights[1, cols, :]
        )
        return carry

    lax.fori_loop(0, 4, source_tile, 0)
    dq_total = dq_acc[me_t] * scale
    for t in t_peers:
        remote(dq_in.at[t], dq_in.at[t], dq_s.at[t], dq_r.at[t], t_dev(t)).wait_recv()
        dq_total += dq_in[t].astype(F32)
    for h in range(heads):
        low = h % per_chunk * rows
        block = dq_total[h // per_chunk, :, low : low + rows]
        dq_ref[:, h * HEAD_DIM : (h + 1) * HEAD_DIM] = block.T

    for c in range(chunks):
        on_line(lambda t, sems, c=c: q_copy(me_t, t, c, sems).wait_send())
        for j in range(tgt_n - 1):
            @pl.when(inner)
            def _(j=j, c=c):
                forward(j, c, lambda copy: copy.wait_send())
    for t in t_peers:
        stat_copy(t).wait_send()
        dq_copy(t).wait_send()
    for h in range(HALVES):
        kv_copy(me_s, x_s, h, kvx_s).wait_send()
        kv_copy(me_s, y_s, h, kvy_s).wait_send()
        relayed = (y_s, x_s) if h == 0 else (x_s, y_s)
        kv_copy(*relayed, h, rkv_s).wait_send()
    for i in range(2):
        for h in range(HALVES):
            via_copy(i, h).wait_send()
            for n in range(2):
                g_copy(i, n, h).wait_send()
    for i in i_peers:
        for p in range(pieces):
            a_copy(p, i).wait_send()
        remote(b2_out.at[i], b2_in.at[i], b2_s.at[i], b2_r.at[i], i_dev(i)).wait_send()
    for o in o_peers:
        remote(b_out.at[o], b_in.at[o], b_s.at[o], b_r.at[o], o_dev(o)).wait_send()
        for p in range(pieces):
            a2_copy(p, o).wait_send()
    for p in tp_peers:
        for i in range(2):
            remote(
                tp_own.at[i], tp_in.at[p, i], tp_s.at[p, i], tp_r.at[p, i], tp_dev(p)
            ).wait_send()

    total = b2_own[me_i]
    for i in i_peers:
        remote(b2_in.at[i], b2_in.at[i], b2_s.at[i], b2_r.at[i], i_dev(i)).wait_recv()
        total += b2_in[i].astype(F32)
    kg_ref[:, pieces * cut :] = total
    for p in range(pieces):
        total = a2_own[p, me_o]
        for o in o_peers:
            remote(
                a2_in.at[p, o], a2_in.at[p, o], a2_s.at[p, o], a2_r.at[p, o], o_dev(o)
            ).wait_recv()
            total += a2_in[p, o].astype(F32)
        kg_ref[:, p * cut : (p + 1) * cut] = total


def finish(*refs):
    *refs, sem = refs
    copies = [
        pltpu.make_async_copy(value, out, sem.at[n])
        for n, (value, out) in enumerate(zip(refs[:3], refs[3:]))
    ]
    for copy in copies:
        copy.start()
    for copy in copies:
        copy.wait()


def shards(
    tgt_n, src_n, tp_n,
    queries, attn_out, out_grad, row_lse, source, saved_keys, saved_values, key_weight, value_weight
):
    heads = row_lse.shape[1]
    rows, width = queries.shape
    src_rows, columns = source.shape
    kv_width = KV_HEADS * HEAD_DIM
    sp_n = tgt_n * src_n
    part = kv_width // sp_n
    key_n, key_m = src_n, tgt_n
    chunks = math.gcd(heads, 2)
    stacked = heads // chunks * rows
    cut = columns // (PIECES + 1) // HEAD_DIM * HEAD_DIM
    rest = columns - PIECES * cut
    dma = pltpu.SemaphoreType.DMA
    vmem = pl.BlockSpec(memory_space=pltpu.VMEM)
    hbm = pl.BlockSpec(memory_space=pltpu.HBM)
    scratch = [
        pltpu.VMEM((src_rows, 2 * kv_width), BF16),
        pltpu.VMEM((2, columns, kv_width), BF16),
        pltpu.VMEM((rows, width), BF16),
        pltpu.VMEM((heads, rows), F32),
        pltpu.VMEM((tgt_n, chunks, 2, rows, width // chunks), BF16),
        pltpu.VMEM((tgt_n, 8, stacked), F32),
        pltpu.VMEM((src_n, HALVES, 2, src_rows // HALVES, HEAD_DIM), BF16),
        pltpu.VMEM((src_n, src_rows, HEAD_DIM), F32),
        pltpu.VMEM((src_n, src_rows, HEAD_DIM), F32),
        pltpu.VMEM((tgt_n, chunks, HEAD_DIM, stacked), F32),
        pltpu.VMEM((tgt_n, chunks, HEAD_DIM, stacked), BF16),
        pltpu.VMEM((tgt_n, chunks, HEAD_DIM, stacked), BF16),
        pltpu.VMEM((2, HALVES, src_rows // HALVES, HEAD_DIM), BF16),
        pltpu.VMEM((2, HALVES, src_rows // HALVES, HEAD_DIM), BF16),
        pltpu.VMEM((2, 2, HALVES, src_rows // HALVES, HEAD_DIM), BF16),
        pltpu.VMEM((2, 2, HALVES, src_rows // HALVES, HEAD_DIM), BF16),
        pltpu.VMEM((2, src_rows, HEAD_DIM), BF16),
        pltpu.VMEM((tp_n, 2, src_rows, HEAD_DIM), BF16),
        pltpu.VMEM((src_rows, columns), BF16),
        pltpu.VMEM((PIECES, key_n, key_m, part, cut), BF16),
        pltpu.VMEM((PIECES, key_n, key_m, part, cut), BF16),
        pltpu.VMEM((PIECES, key_m, part, cut), F32),
        pltpu.VMEM((PIECES, key_m, part, cut), BF16),
        pltpu.VMEM((PIECES, key_m, part, cut), BF16),
        pltpu.VMEM((key_m, key_n, part, rest), BF16),
        pltpu.VMEM((key_m, key_n, part, rest), BF16),
        pltpu.VMEM((key_n, part, rest), F32),
        pltpu.VMEM((key_n, part, rest), BF16),
        pltpu.VMEM((key_n, part, rest), BF16),
        dma((3,)),
        dma((2 * HALVES,)),
        dma((chunks, 2)),
        dma((2,)),
    ]
    for shape in (
        (tgt_n, chunks), (tgt_n, chunks), (tgt_n, chunks), (tgt_n,), (tgt_n,),
        (HALVES,), (HALVES,), (src_n, HALVES), (HALVES,), (tgt_n,), (tgt_n,),
        (2, HALVES), (2, HALVES), (2, 2, HALVES), (2, 2, HALVES),
        (tp_n, 2), (tp_n, 2), (PIECES, key_n), (PIECES, key_n), (PIECES, key_m), (PIECES, key_m),
        (key_m,), (key_m,), (key_n,), (key_n,),
    ):
        scratch.append(dma(shape))
    shapes = ((rows, width), (src_rows, columns), (part, columns))
    grads = pl.pallas_call(
        functools.partial(kernel, tgt_n, src_n, key_n, tp_n, src_rows * sp_n),
        out_shape=[pltpu.VMEM(shape, F32) for shape in shapes],
        in_specs=[hbm] * 9,
        out_specs=[vmem] * 3,
        scratch_shapes=scratch,
        compiler_params=pltpu.CompilerParams(
            collective_id=0, has_side_effects=True,
            vmem_limit_bytes=VMEM_BYTES - 4 * sum(map(math.prod, shapes)),
        ),
        name="attention_grads",
    )(
        queries, attn_out, out_grad, row_lse.T, saved_keys, saved_values, source,
        key_weight, value_weight,
    )
    return tuple(pl.pallas_call(
        finish,
        out_shape=[jax.ShapeDtypeStruct(shape, F32) for shape in shapes],
        in_specs=[vmem] * 3,
        out_specs=[hbm] * 3,
        scratch_shapes=[dma((3,))],
        compiler_params=pltpu.CompilerParams(vmem_limit_bytes=2**20),
        name="write_grads",
    )(*grads))


def solution(mesh):
    sp_n, tp_n = mesh.shape["sp"], mesh.shape["tp"]
    src_n = math.gcd(sp_n, 4)
    in_specs = (
        P("sp", "tp"),
        P("sp", "tp"),
        P("sp", "tp"),
        P("sp", "tp"),
        P("sp", "tp"),
        P("sp", None),
        P("sp", None),
        P("tp", None),
        P("tp", None),
    )
    out_specs = (P("sp", "tp"), P("sp", "tp"), P("sp", "tp"))
    return jax.shard_map(
        functools.partial(shards, sp_n // src_n, src_n, tp_n),
        mesh=mesh, in_specs=in_specs, out_specs=out_specs, check_vma=False,
    )
```

time: 61.3 us -> 53.3 us (0.87)
  Pallas kernels: 60.6 us -> 52.5 us
    pallas_call x1, Pallas kernels: 58.4 us -> 50.3 us  [shards(): pl.pallas_call(functools.partial(kernel, tgt_n, src_n, key_n, tp_n, src_r...]
where the time goes in v2:
time: 53.3 us; the launch traced here: 53.1 us
  Pallas kernels  52.5 us (98%)
  between operations  0.64 us (1%)
    pallas_call x1, Pallas kernels, shards(): pl.pallas_call(functools.partial(kernel, tgt_n, src_n, key_n, tp_n, src_r...  50.3 us
    pallas_call x1, Pallas kernels, shards(): pl.pallas_call(finish, out_shape=[jax.ShapeDtypeStruct(shape, F32) for sh...  2.15 us

profile of v2, /device:TPU:0, one launch (start us, length us, event | category | flops | bytes accessed | tf_op | source)
XLA Modules:
  0.0 53.1 jit_solution(798307285935164189)
XLA Ops:
  0.6 50.3 %attention_grads.1 = (f32[128,512]{1,0:T(8,128)S(1)}, f32[512,2048]{1,0:T(8,128)S(1)}, f32[16,2048]{1,0:T(8,128)S(1)}) custom-call(bf16[128,512]{1,0:T(8,128)(2,1)} %q_hbm.1, bf16[128,512]{1,0:T(8,128)(2,1)} %o_hbm.1, bf16[128,512]{1,0:T(8,128)(2,1)} %d_hbm.1, f32[4,128]{1,0:T(4,128)} %bitcast.1, bf16[512,256]{1,0:T(8,128)(2,1)} %key_hbm.1, ...), custom_call_target="tpu_custom_call" | custom-call | tf_op jit(solution)/shard_map/attention_grads/pallas_call | solution.py:572
  50.9 2.1 %write_grads.1 = (f32[128,512]{1,0:T(8,128)}, f32[512,2048]{1,0:T(8,128)}, f32[16,2048]{1,0:T(8,128)}) custom-call(f32[128,512]{1,0:T(8,128)S(1)} %get-tuple-element.6.refs_0_, f32[512,2048]{1,0:T(8,128)S(1)} %get-tuple-element.7.refs_1_, f32[16,2048]{1,0:T(8,128)S(1)} %get-tuple-element.8.refs_2_), custom_call_target="tpu_custom_call" | custom-call | tf_op jit(solution)/shard_map/write_grads/pallas_call | solution.py:587

commit v3 on v2

--- a/solution.py
+++ b/solution.py
@@ -40,8 +40,8 @@
     dq_ref, sg_ref, kg_ref,
     kv_ref, weights,    o_own, lse_own, qd, stats, kvs, dk, dv, dq_acc, dq_out, dq_in, d_out, g_via, g_out, g_in, tp_own, tp_in,
     src, a_out, a_in, a2_own, a2_out, a2_in, b_out, b_in, b2_own, b2_out, b2_in,
-    copy_sem, load_kv, load_q, load_o, up_s, down_s, qd_r, st_s, st_r, kvx_s, kvy_s, kv_r, rkv_s, dq_s, dq_r, via_s, via_r, g_s, g_r, tp_s, tp_r,
-    a_s, a_r, a2_s, a2_r, b_s, b_r, b2_s, b2_r,
+    copy_sem, load_kv, load_q, load_o, q_s, q_down, st_s, st_down, kv_s, dq_s, via_s, g_s, tp_s, a_s, a2_s, b_s, b2_s,
+    qd_r, st_r, kv_r, dq_r, via_r, g_r, tp_r, a_r, a2_r, b_r, b2_r,
 ):
     sp = lax.axis_index("sp")
     tp = lax.axis_index("tp")
@@ -67,7 +67,7 @@
     heads = q_hbm.shape[1] // HEAD_DIM
     chunks = qd.shape[1]
     src_rows = dk.shape[1]
-    stacked = stats.shape[2]
+    stacked = dq_acc.shape[3]
     split = (chunks + 1) // 2
     per_chunk = heads // chunks
     per_key = HEADS // KV_HEADS
@@ -82,91 +82,107 @@
 
     o_dev, i_dev = t_dev, s_dev
 
+    def drain(ref, sem):
+        pltpu.make_async_copy(ref, ref, sem).wait()
+
     def tp_dev(p):
         return {"sp": sp, "tp": p}
 
-    def remote(source, target, send, recv, device):
+    def remote(source, target, sent, recv, device):
         return pltpu.make_async_remote_copy(
-            src_ref=source, dst_ref=target, send_sem=send, recv_sem=recv,
+            src_ref=source, dst_ref=target, send_sem=sent, recv_sem=recv,
             device_id=device, device_id_type=MESH,
         )
 
-    partners = (
-        [t_dev(t) for t in t_peers] + [s_dev(s) for s in s_peers] + [tp_dev(p) for p in tp_peers]
-    )
     barrier = pltpu.get_barrier_semaphore()
-    for device in partners:
+    def greet(device):
         pl.semaphore_signal(barrier, inc=1, device_id=device, device_id_type=MESH)
+
+    for s in (x_s, y_s):
+        greet(s_dev(s))
+    for p in tp_peers:
+        greet(tp_dev(p))
+
+    @pl.when(above > 0)
+    def _():
+        greet(t_dev(me_t + 1))
+
+    @pl.when(below > 0)
+    def _():
+        greet(t_dev(me_t - 1))
+
     piece = src_rows // HALVES
     chunk_w = per_chunk * HEAD_DIM
-    loads = []
+    kv_loads = [
+        pltpu.make_async_copy(
+            ref.at[pl.ds(h * piece, piece), pl.ds(kv_col, HEAD_DIM)],
+            kvs.at[me_s, h, i], load_kv,
+        )
+        for h in range(HALVES) for i, ref in enumerate((key_hbm, value_hbm))
+    ]
+    q_loads = [
+        pltpu.make_async_copy(
+            ref.at[:, pl.ds(c * chunk_w, chunk_w)], qd.at[me_t, c, i], load_q.at[c]
+        )
+        for c in range(chunks) for i, ref in enumerate((q_hbm, d_hbm))
+    ]
+    loads = [
+        pltpu.make_async_copy(o_hbm, o_own, load_o.at[0]),
+        pltpu.make_async_copy(lse_hbm, lse_own, load_o.at[1]),
+    ]
+    late = [pltpu.make_async_copy(source_hbm, src, copy_sem.at[0])]
+    for i, ref in enumerate((kw_hbm, vw_hbm)):
+        late.append(pltpu.make_async_copy(ref, weights.at[i], copy_sem.at[1 + i]))
+    for copy in kv_loads + q_loads + loads:
+        copy.start()
+
+    def q_copy(block, t, c, sem):
+        return remote(qd.at[block, c], qd.at[block, c], sem, qd_r.at[block, c], t_dev(t))
+
+    def kv_copy(block, s, h):
+        return remote(kvs.at[block, h], kvs.at[block, h], kv_s, kv_r.at[block, h], s_dev(s))
+
+    def stat_copy(block, t, sem):
+        return remote(stats.at[block], stats.at[block], sem, st_r.at[block], t_dev(t))
+
+    def on_line(act):
+        @pl.when(above > 0)
+        def _():
+            act(me_t + 1, q_s.at[me_t], st_s.at[me_t])
+
+        @pl.when(below > 0)
+        def _():
+            act(me_t - 1, q_down, st_down)
+
+    sides = jnp.minimum(above, 1) + jnp.minimum(below, 1)
+    pl.semaphore_wait(barrier, sides + 1 + tp_n)
+    drain(qd.at[me_t, 0], load_q.at[0])
+    on_line(lambda t, q, st: q_copy(me_t, t, 0, q).start())
+    drain(kvs.at[me_s], load_kv)
     for h in range(HALVES):
-        for i, ref in enumerate((key_hbm, value_hbm)):
-            loads.append(pltpu.make_async_copy(
-                ref.at[pl.ds(h * piece, piece), pl.ds(kv_col, HEAD_DIM)],
-                kvs.at[me_s, h, i], load_kv.at[2 * h + i],
-            ))
-    for c in range(chunks):
-        for i, ref in enumerate((q_hbm, d_hbm)):
-            loads.append(pltpu.make_async_copy(
-                ref.at[:, pl.ds(c * chunk_w, chunk_w)], qd.at[me_t, c, i], load_q.at[c, i]
-            ))
-    loads.append(pltpu.make_async_copy(o_hbm, o_own, load_o.at[0]))
-    loads.append(pltpu.make_async_copy(lse_hbm, lse_own, load_o.at[1]))
-    lates = [pltpu.make_async_copy(source_hbm, src, copy_sem.at[0])]
-    for i, ref in enumerate((kw_hbm, vw_hbm)):
-        lates.append(pltpu.make_async_copy(ref, weights.at[i], copy_sem.at[1 + i]))
-    for copy in loads:
-        copy.start()
-    dk[...] = jnp.zeros_like(dk)
-    dv[...] = jnp.zeros_like(dv)
-    dq_acc[...] = jnp.zeros_like(dq_acc)
+        kv_copy(me_s, x_s, HALVES - 1 - h).start()
+        kv_copy(me_s, y_s, h).start()
+    for c in range(1, chunks):
+        drain(qd.at[me_t, c], load_q.at[c])
     for copy in loads:
         copy.wait()
     ones = jnp.ones((8, HEAD_DIM), F32)
     for h in range(heads):
         cols = pl.ds(h * HEAD_DIM, HEAD_DIM)
-        c, span = h // per_chunk, pl.ds(h % per_chunk * rows, rows)
+        c = h // per_chunk
         grad = qd[me_t, c, 1, :, pl.ds(h % per_chunk * HEAD_DIM, HEAD_DIM)]
         prod = grad.astype(F32) * o_own[:, cols].astype(F32)
         delta = dot_nt(ones, prod, lax.Precision.HIGHEST)
-        stats[me_t, 2 * c : 2 * c + 1, span] = lse_own[h : h + 1, :] * LOG2E
-        stats[me_t, 2 * c + 1 : 2 * c + 2, span] = delta[0:1, :]
-    pl.semaphore_wait(barrier, len(partners))
-    for copy in lates:
+        stats[me_t, h : h + 1] = lse_own[h : h + 1, :] * LOG2E
+        stats[me_t, heads + h : heads + h + 1] = delta[0:1, :]
+    on_line(lambda t, q, st: stat_copy(me_t, t, st).start())
+    for c in range(1, chunks):
+        on_line(lambda t, q, st, c=c: q_copy(me_t, t, c, q).start())
+    for copy in late:
         copy.start()
-
-    def q_copy(block, t, c, sems):
-        return remote(
-            qd.at[block, c], qd.at[block, c], sems.at[block, c], qd_r.at[block, c], t_dev(t)
-        )
-
-    def kv_copy(block, s, h, sems):
-        return remote(
-            kvs.at[block, h], kvs.at[block, h], sems.at[h], kv_r.at[block, h], s_dev(s)
-        )
-
-    def stat_copy(t):
-        return remote(stats.at[me_t], stats.at[me_t], st_s.at[t], st_r.at[me_t], t_dev(t))
-
-    def on_line(act):
-        @pl.when(above > 0)
-        def _():
-            act(me_t + 1, up_s)
-
-        @pl.when(below > 0)
-        def _():
-            act(me_t - 1, down_s)
-
-    for n in range(max(HALVES, chunks)):
-        if n < HALVES:
-            kv_copy(me_s, x_s, HALVES - 1 - n, kvx_s).start()
-            kv_copy(me_s, y_s, n, kvy_s).start()
-        if n < chunks:
-            on_line(lambda t, sems, n=n: q_copy(me_t, t, n, sems).start())
-        if n == 0:
-            for t in t_peers:
-                stat_copy(t).start()
+    dk[...] = jnp.zeros_like(dk)
+    dv[...] = jnp.zeros_like(dv)
+    dq_acc[...] = jnp.zeros_like(dq_acc)
 
     def stack(t, i, low, high):
         return jnp.concatenate(
@@ -178,7 +194,9 @@
         )
 
     def stat(t, i, low, high):
-        return jnp.concatenate([stats[t, 2 * c + i : 2 * c + i + 1, :] for c in range(low, high)], axis=1)
+        first = i * heads + low * per_chunk
+        count = (high - low) * per_chunk
+        return jnp.concatenate([stats[t, first + h : first + h + 1] for h in range(count)], axis=1)
 
     def keys(s, i):
         return kvs[s, :, i].reshape(src_rows, HEAD_DIM)
@@ -201,36 +219,41 @@
             dq_acc[t, c] += part_q[:, span : span + stacked]
 
     def got_q(j, c):
-        q_copy(order[j], me_t, c, up_s).wait_recv()
-
-    def forward(j, c, act):
+        q_copy(order[j], me_t, c, q_down).wait_recv()
+
+    def forward(j, act):
         @pl.when(order[j] > me_t)
         def _():
-            act(q_copy(order[j], me_t - 1, c, down_s))
+            act(me_t - 1)
 
         @pl.when(order[j] < me_t)
         def _():
-            act(q_copy(order[j], me_t + 1, c, up_s))
+            act(me_t + 1)
 
     def pass_q(j, c):
         @pl.when(inner)
         def _():
             got_q(j, c)
-            forward(j, c, lambda copy: copy.start())
+            forward(j, lambda t: q_copy(order[j], t, c, q_s.at[order[j]]).start())
+            if c == split - 1:
+                got_stats(order[j])
+                forward(j, lambda t: stat_copy(order[j], t, st_s.at[order[j]]).start())
 
     def last_q(j, c):
         @pl.when(jnp.logical_not(inner))
         def _():
             got_q(j, c)
+            if c == split - 1:
+                got_stats(order[j])
 
     def got_stats(t):
-        remote(stats.at[t], stats.at[t], st_s.at[t], st_r.at[t], t_dev(t)).wait_recv()
+        stat_copy(t, me_t, st_down).wait_recv()
 
     def got_kv(s, h):
-        kv_copy(s, s, h, kvx_s).wait_recv()
+        kv_copy(s, s, h).wait_recv()
 
     def dq_copy(t):
-        return remote(dq_out.at[t], dq_in.at[me_t], dq_s.at[t], dq_r.at[me_t], t_dev(t))
+        return remote(dq_out.at[t], dq_in.at[me_t], dq_s, dq_r, t_dev(t))
 
     def g_part(s, i, h):
         span = pl.ds(h * piece, piece)
@@ -238,12 +261,12 @@
 
     def via_copy(i, h):
         return remote(
-            d_out.at[i, h], g_via.at[i, h], via_s.at[i, h], via_r.at[i, h], s_dev((x_s, y_s)[h])
+            d_out.at[i, h], g_via.at[i, h], via_s, via_r.at[i, h], s_dev((x_s, y_s)[h])
         )
 
     def g_copy(i, n, h):
         return remote(
-            g_out.at[i, n, h], g_in.at[i, n, h], g_s.at[i, n, h], g_r.at[i, n, h],
+            g_out.at[i, n, h], g_in.at[i, n, h], g_s, g_r.at[i],
             s_dev((x_s, y_s)[n]),
         )
 
@@ -268,18 +291,25 @@
         dq_out[t] = (dq_acc[t] * scale).astype(BF16)
         dq_copy(t).start()
 
+    def edge(t):
+        return inner & ((t == 0) | (t == tgt_n - 1))
+
+    def early_dq(t):
+        @pl.when(jnp.logical_not(edge(t)))
+        def _():
+            send_dq(t)
+
     everyone = [me_s, x_s, y_s, d_s]
     tile(me_t, me_s)
     got_kv(y_s, 0)
-    kv_copy(y_s, x_s, 0, rkv_s).start()
+    kv_copy(y_s, x_s, 0).start()
     for h in range(1, HALVES):
         got_kv(x_s, h)
-        kv_copy(x_s, y_s, h, rkv_s).start()
+        kv_copy(x_s, y_s, h).start()
     for c in range(split):
         pass_q(0, c)
         last_q(0, c)
         pass_q(1, c)
-    got_stats(order[0])
     tile(order[0], me_s, 0, split)
     for h in range(1, HALVES):
         got_kv(y_s, h)
@@ -299,17 +329,15 @@
     tile(order[0], y_s)
     for t in (me_t, order[0]):
         tile(t, d_s)
-    send_dq(order[0])
+    early_dq(order[0])
     for c in range(split, chunks):
         pass_q(2, c)
-    got_stats(order[1])
     for c in range(chunks):
         last_q(1, c)
     for s in everyone:
         tile(order[1], s)
-    send_dq(order[1])
+    early_dq(order[1])
     for j in range(2, tgt_n - 1):
-        got_stats(order[j])
         for c in range(chunks):
             if j > 2:
                 pass_q(j, c)
@@ -320,7 +348,7 @@
         if j < tgt_n - 2:
             for s in everyone:
                 tile(order[j], s, split, chunks)
-            send_dq(order[j])
+            early_dq(order[j])
     for n, s in enumerate([d_s, x_s, y_s, me_s]):
         tile(order[-1], s, split, chunks)
         if n == 0:
@@ -328,29 +356,31 @@
         elif n < 3:
             send_plain(0, n - 1)
     send_dq(order[-1])
+    for t in order[:-1]:
+        @pl.when(edge(t))
+        def _(t=t):
+            send_dq(t)
+
     send_sum(0)
     send_via(1)
     for n in range(2):
         send_plain(1, n)
 
     def reduce_g(i):
+        drain(g_in.at[i], g_r.at[i])
         for h in range(HALVES):
             total = g_part(me_s, i, h)
             for n in range(2):
-                g_copy(i, n, h).wait_recv()
                 total += g_in[i, n, h].astype(F32)
             tp_own[i, h * piece : (h + 1) * piece] = total.astype(BF16)
         for p in tp_peers:
             remote(
-                tp_own.at[i], tp_in.at[tp, i], tp_s.at[p, i], tp_r.at[tp, i], tp_dev(p)
+                tp_own.at[i], tp_in.at[tp, i], tp_s, tp_r.at[i], tp_dev(p)
             ).start()
         tp_in[tp, i] = tp_own[i]
 
     def gather_g(i):
-        for p in tp_peers:
-            remote(
-                tp_in.at[p, i], tp_in.at[p, i], tp_s.at[p, i], tp_r.at[p, i], tp_dev(p)
-            ).wait_recv()
+        drain(tp_in.at[0 : tp_n - 1, i], tp_r.at[i])
         for g in range(KV_HEADS):
             owners = [p for p in range(tp_n) if p * heads // per_key == g]
             half = tp_in[owners[0], i]
@@ -362,7 +392,7 @@
             kv_ref[:, pl.ds((i * KV_HEADS + g) * HEAD_DIM, HEAD_DIM)] = half
 
     reduce_g(0)
-    lates[0].wait()
+    late[0].wait()
     gather_g(0)
     pieces, part, cut = a2_own.shape[0], a2_own.shape[2], a2_own.shape[3]
     key_half = kv_ref[:, 0 : KV_HEADS * HEAD_DIM]
@@ -370,12 +400,12 @@
 
     def a_copy(p, i):
         return remote(
-            a_out.at[p, i], a_in.at[p, me_i], a_s.at[p, i], a_r.at[p, me_i], i_dev(i)
+            a_out.at[p, i], a_in.at[p, me_i], a_s, a_r.at[p], i_dev(i)
         )
 
     def a2_copy(p, o):
         return remote(
-            a2_out.at[p, o], a2_in.at[p, me_o], a2_s.at[p, o], a2_r.at[p, me_o], o_dev(o)
+            a2_out.at[p, o], a2_in.at[p, me_o], a2_s, a2_r, o_dev(o)
         )
 
     def a_part(p):
@@ -394,103 +424,91 @@
             low = (o * key_n + i) * part
             b_out[o, i] = partial[low : low + part].astype(BF16)
     for o in o_peers:
-        remote(b_out.at[o], b_in.at[me_o], b_s.at[o], b_r.at[me_o], o_dev(o)).start()
+        remote(b_out.at[o], b_in.at[me_o], b_s, b_r, o_dev(o)).start()
     for p in range(1, pieces):
         a_part(p)
     send_sum(1)
 
+    def add_source(i):
+        width = KV_HEADS * HEAD_DIM
+        span = sg_ref.shape[1] // 4
+
+        def body(n, carry):
+            cols = pl.ds(pl.multiple_of(n * span, HEAD_DIM), span)
+            term = dot_nt(kv_ref[:, i * width : (i + 1) * width], weights[i, cols, :])
+            sg_ref[:, cols] = sg_ref[:, cols] + term if i else term
+            return carry
+
+        lax.fori_loop(0, 4, body, 0)
+
     def a_sum(p):
         total = a_out[p, me_i].astype(F32)
+        drain(a_in.at[p, 0 : key_n - 1], a_r.at[p])
         for i in i_peers:
-            remote(
-                a_in.at[p, i], a_in.at[p, i], a_s.at[p, i], a_r.at[p, i], i_dev(i)
-            ).wait_recv()
             total += a_in[p, i].astype(F32)
         a2_own[p] = total
         a2_out[p] = total.astype(BF16)
         for o in o_peers:
             a2_copy(p, o).start()
 
+    for copy in late[1:]:
+        copy.wait()
+    add_source(0)
     a_sum(0)
     total = b_out[me_o].astype(F32)
+    drain(b_in.at[0 : key_m - 1], b_r)
     for o in o_peers:
-        remote(b_in.at[o], b_in.at[o], b_s.at[o], b_r.at[o], o_dev(o)).wait_recv()
         total += b_in[o].astype(F32)
     b2_own[...] = total
     b2_out[...] = total.astype(BF16)
     for i in i_peers:
-        remote(b2_out.at[i], b2_in.at[me_i], b2_s.at[i], b2_r.at[me_i], i_dev(i)).start()
+        remote(b2_out.at[i], b2_in.at[me_i], b2_s, b2_r, i_dev(i)).start()
     for p in range(1, pieces):
         a_sum(p)
 
     reduce_g(1)
     gather_g(1)
-    for copy in lates[1:]:
-        copy.wait()
-    kv_width = KV_HEADS * HEAD_DIM
-    span = sg_ref.shape[1] // 4
-
-    def source_tile(n, carry):
-        cols = pl.ds(pl.multiple_of(n * span, HEAD_DIM), span)
-        sg_ref[:, cols] = dot_nt(kv_ref[:, :kv_width], weights[0, cols, :]) + dot_nt(
-            kv_ref[:, kv_width:], weights[1, cols, :]
-        )
-        return carry
-
-    lax.fori_loop(0, 4, source_tile, 0)
+    add_source(1)
     dq_total = dq_acc[me_t] * scale
+    drain(dq_in.at[0 : tgt_n - 1], dq_r)
     for t in t_peers:
-        remote(dq_in.at[t], dq_in.at[t], dq_s.at[t], dq_r.at[t], t_dev(t)).wait_recv()
         dq_total += dq_in[t].astype(F32)
     for h in range(heads):
         low = h % per_chunk * rows
         block = dq_total[h // per_chunk, :, low : low + rows]
         dq_ref[:, h * HEAD_DIM : (h + 1) * HEAD_DIM] = block.T
 
-    for c in range(chunks):
-        on_line(lambda t, sems, c=c: q_copy(me_t, t, c, sems).wait_send())
-        for j in range(tgt_n - 1):
-            @pl.when(inner)
-            def _(j=j, c=c):
-                forward(j, c, lambda copy: copy.wait_send())
-    for t in t_peers:
-        stat_copy(t).wait_send()
-        dq_copy(t).wait_send()
-    for h in range(HALVES):
-        kv_copy(me_s, x_s, h, kvx_s).wait_send()
-        kv_copy(me_s, y_s, h, kvy_s).wait_send()
-        relayed = (y_s, x_s) if h == 0 else (x_s, y_s)
-        kv_copy(*relayed, h, rkv_s).wait_send()
-    for i in range(2):
-        for h in range(HALVES):
-            via_copy(i, h).wait_send()
-            for n in range(2):
-                g_copy(i, n, h).wait_send()
+    def done_line(t, q, st):
+        drain(qd.at[me_t], q)
+        drain(stats.at[me_t], st)
+
+    on_line(done_line)
+
+    @pl.when(inner)
+    def _():
+        for t in order:
+            drain(qd.at[t], q_s.at[t])
+            drain(stats.at[t], st_s.at[t])
+
+    drain(kvs.at[0 : src_n - 1], kv_s)
+    drain(dq_out.at[0 : tgt_n - 1], dq_s)
+    drain(d_out, via_s)
+    drain(g_out, g_s)
+    drain(tp_in.at[0 : tp_n - 1], tp_s)
+    drain(a_out.at[:, 0 : key_n - 1], a_s)
+    drain(a2_out.at[:, 0 : key_m - 1], a2_s)
+    drain(b_out.at[0 : key_m - 1], b_s)
+    drain(b2_out.at[0 : key_n - 1], b2_s)
+
+    total = b2_own[me_i]
+    drain(b2_in.at[0 : key_n - 1], b2_r)
     for i in i_peers:
-        for p in range(pieces):
-            a_copy(p, i).wait_send()
-        remote(b2_out.at[i], b2_in.at[i], b2_s.at[i], b2_r.at[i], i_dev(i)).wait_send()
-    for o in o_peers:
-        remote(b_out.at[o], b_in.at[o], b_s.at[o], b_r.at[o], o_dev(o)).wait_send()
-        for p in range(pieces):
-            a2_copy(p, o).wait_send()
-    for p in tp_peers:
-        for i in range(2):
-            remote(
-                tp_own.at[i], tp_in.at[p, i], tp_s.at[p, i], tp_r.at[p, i], tp_dev(p)
-            ).wait_send()
-
-    total = b2_own[me_i]
-    for i in i_peers:
-        remote(b2_in.at[i], b2_in.at[i], b2_s.at[i], b2_r.at[i], i_dev(i)).wait_recv()
         total += b2_in[i].astype(F32)
     kg_ref[:, pieces * cut :] = total
+    drain(a2_in.at[:, 0 : key_m - 1], a2_r)
     for p in range(pieces):
         total = a2_own[p, me_o]
         for o in o_peers:
-            remote(
-                a2_in.at[p, o], a2_in.at[p, o], a2_s.at[p, o], a2_r.at[p, o], o_dev(o)
-            ).wait_recv()
             total += a2_in[p, o].astype(F32)
         kg_ref[:, p * cut : (p + 1) * cut] = total
 
@@ -531,7 +549,7 @@
         pltpu.VMEM((rows, width), BF16),
         pltpu.VMEM((heads, rows), F32),
         pltpu.VMEM((tgt_n, chunks, 2, rows, width // chunks), BF16),
-        pltpu.VMEM((tgt_n, 8, stacked), F32),
+        pltpu.VMEM((tgt_n, 2 * heads, rows), F32),
         pltpu.VMEM((src_n, HALVES, 2, src_rows // HALVES, HEAD_DIM), BF16),
         pltpu.VMEM((src_n, src_rows, HEAD_DIM), F32),
         pltpu.VMEM((src_n, src_rows, HEAD_DIM), F32),
@@ -556,16 +574,14 @@
         pltpu.VMEM((key_n, part, rest), BF16),
         pltpu.VMEM((key_n, part, rest), BF16),
         dma((3,)),
-        dma((2 * HALVES,)),
-        dma((chunks, 2)),
+        dma(()),
+        dma((chunks,)),
         dma((2,)),
     ]
     for shape in (
-        (tgt_n, chunks), (tgt_n, chunks), (tgt_n, chunks), (tgt_n,), (tgt_n,),
-        (HALVES,), (HALVES,), (src_n, HALVES), (HALVES,), (tgt_n,), (tgt_n,),
-        (2, HALVES), (2, HALVES), (2, 2, HALVES), (2, 2, HALVES),
-        (tp_n, 2), (tp_n, 2), (PIECES, key_n), (PIECES, key_n), (PIECES, key_m), (PIECES, key_m),
-        (key_m,), (key_m,), (key_n,), (key_n,),
+        (tgt_n,), (), (tgt_n,), (), (), (), (), (), (), (), (), (), (),
+        (tgt_n, chunks), (tgt_n,), (src_n, HALVES), (), (2, HALVES), (2,), (2,), (PIECES,),
+        (), (), (),
     ):
         scratch.append(dma(shape))
     shapes = ((rows, width), (src_rows, columns), (part, columns))

time: 53.3 us -> 49.5 us (0.929)
  Pallas kernels: 52.5 us -> 48.7 us
    pallas_call x1, Pallas kernels: 50.3 us -> 46.5 us  [shards(): pl.pallas_call(functools.partial(kernel, tgt_n, src_n, key_n, tp_n, src_r...]
where the time goes in v3:
time: 49.5 us; the launch traced here: 49.3 us
  Pallas kernels  48.7 us (98%)
  between operations  0.64 us (1%)
    pallas_call x1, Pallas kernels, shards(): pl.pallas_call(functools.partial(kernel, tgt_n, src_n, key_n, tp_n, src_r...  46.5 us
    pallas_call x1, Pallas kernels, shards(): pl.pallas_call(finish, out_shape=[jax.ShapeDtypeStruct(shape, F32) for sh...  2.15 us

profile of v3, /device:TPU:0, one launch (start us, length us, event | category | flops | bytes accessed | tf_op | source)
XLA Modules:
  0.0 49.3 jit_solution(18257399978749665839)
XLA Ops:
  0.6 46.5 %attention_grads.1 = (f32[128,512]{1,0:T(8,128)S(1)}, f32[512,2048]{1,0:T(8,128)S(1)}, f32[16,2048]{1,0:T(8,128)S(1)}) custom-call(bf16[128,512]{1,0:T(8,128)(2,1)} %q_hbm.1, bf16[128,512]{1,0:T(8,128)(2,1)} %o_hbm.1, bf16[128,512]{1,0:T(8,128)(2,1)} %d_hbm.1, f32[4,128]{1,0:T(4,128)} %bitcast.1, bf16[512,256]{1,0:T(8,128)(2,1)} %key_hbm.1, ...), custom_call_target="tpu_custom_call" | custom-call | tf_op jit(solution)/shard_map/attention_grads/pallas_call | solution.py:588
  47.2 2.1 %write_grads.1 = (f32[128,512]{1,0:T(8,128)}, f32[512,2048]{1,0:T(8,128)}, f32[16,2048]{1,0:T(8,128)}) custom-call(f32[128,512]{1,0:T(8,128)S(1)} %get-tuple-element.6.refs_0_, f32[512,2048]{1,0:T(8,128)S(1)} %get-tuple-element.7.refs_1_, f32[16,2048]{1,0:T(8,128)S(1)} %get-tuple-element.8.refs_2_), custom_call_target="tpu_custom_call" | custom-call | tf_op jit(solution)/shard_map/write_grads/pallas_call | solution.py:603

commit v4 on v3

--- a/solution.py
+++ b/solution.py
@@ -332,10 +332,11 @@
     early_dq(order[0])
     for c in range(split, chunks):
         pass_q(2, c)
-    for c in range(chunks):
-        last_q(1, c)
-    for s in everyone:
-        tile(order[1], s)
+    for low, high in ((0, split), (split, chunks)):
+        for c in range(low, high):
+            last_q(1, c)
+        for s in everyone:
+            tile(order[1], s, low, high)
     early_dq(order[1])
     for j in range(2, tgt_n - 1):
         for c in range(chunks):

time: 49.5 us -> 49.5 us (level)
  no operation moved by 1% of the time
where the time goes in v4:
time: 49.5 us; the launch traced here: 49.3 us
  Pallas kernels  48.7 us (98%)
  between operations  0.64 us (1%)
    pallas_call x1, Pallas kernels, shards(): pl.pallas_call(functools.partial(kernel, tgt_n, src_n, key_n, tp_n, src_r...  46.5 us
    pallas_call x1, Pallas kernels, shards(): pl.pallas_call(finish, out_shape=[jax.ShapeDtypeStruct(shape, F32) for sh...  2.15 us

profile of v4, /device:TPU:0, one launch (start us, length us, event | category | flops | bytes accessed | tf_op | source)
XLA Modules:
  0.0 49.3 jit_solution(10050916903971974284)
XLA Ops:
  0.6 46.5 %attention_grads.1 = (f32[128,512]{1,0:T(8,128)S(1)}, f32[512,2048]{1,0:T(8,128)S(1)}, f32[16,2048]{1,0:T(8,128)S(1)}) custom-call(bf16[128,512]{1,0:T(8,128)(2,1)} %q_hbm.1, bf16[128,512]{1,0:T(8,128)(2,1)} %o_hbm.1, bf16[128,512]{1,0:T(8,128)(2,1)} %d_hbm.1, f32[4,128]{1,0:T(4,128)} %bitcast.1, bf16[512,256]{1,0:T(8,128)(2,1)} %key_hbm.1, ...), custom_call_target="tpu_custom_call" | custom-call | tf_op jit(solution)/shard_map/attention_grads/pallas_call | solution.py:589
  47.2 2.1 %write_grads.1 = (f32[128,512]{1,0:T(8,128)}, f32[512,2048]{1,0:T(8,128)}, f32[16,2048]{1,0:T(8,128)}) custom-call(f32[128,512]{1,0:T(8,128)S(1)} %get-tuple-element.6.refs_0_, f32[512,2048]{1,0:T(8,128)S(1)} %get-tuple-element.7.refs_1_, f32[16,2048]{1,0:T(8,128)S(1)} %get-tuple-element.8.refs_2_), custom_call_target="tpu_custom_call" | custom-call | tf_op jit(solution)/shard_map/write_grads/pallas_call | solution.py:604
